TPU v7x, 32 devices: a whole 2x2x4 slice. The times are simulated.
32 devices in a mesh: ep: 4 (over y, x), tp: 8 (over z, core).
Axes of the slice: x: 2, y: 2, z: 4, core: 2. Of those that a mesh axis runs over, the one named last changes fastest.
Arguments:
- scan_source_values: bfloat16 [1024, 8192], P('tp', 'ep'), may hold values from -6 to 6
- switch_path_values: bfloat16 [1024, 8192], P('tp', 'ep'), may hold values from -6 to 6
- causal_filter_coefficients: bfloat16 [1024, 4], replicated, may hold values from -3 to 3
- scan_switch_blockmap: bfloat16 [16, 64, 64], replicated, may hold values from -0.75 to 0.75
- entry_switch_blockmap: bfloat16 [16, 64, 64], replicated, may hold values from -0.75 to 0.75
- feature_fading_speeds: float32 [1024], replicated, may hold values from 0 to 1
- spike_amount: float32 [8192], P('ep'), may hold values from -1 to 0
- final_linear_map: bfloat16 [1024, 2048], replicated, may hold values from -0.1875 to 0.1875
- dispatched_group_activity: bfloat16 [4096, 2048], P(('ep', 'tp')), may hold values from -6 to 6
- specialist_rmsgain: bfloat16 [2048], replicated, may hold values from 0.099609375 to 1.8984375
- selected_specialist_ids: int32 [4096, 2], P(('ep', 'tp')), may hold values from 0 to 3, all different within a row; in each aligned block of 128 rows (0 to 127, 128 to 255, ...) at most 96 rows name the same one
- selected_specialist_share: float32 [4096, 2], P(('ep', 'tp')), may hold values from 0.2 to 1
- specialist_switch_maps: bfloat16 [4, 2048, 2048], P('ep', None, 'tp'), may hold values from -0.3125 to 0.3125
- specialist_widen_maps: bfloat16 [4, 2048, 2048], P('ep', None, 'tp'), may hold values from -0.3125 to 0.3125
- specialist_shrink_maps: bfloat16 [4, 2048, 2048], P('ep', None, 'tp'), may hold values from -0.03125 to 0.03125
Outputs:
- scan_path_result: bfloat16 [8192, 2048], P(('ep', 'tp'))
- moe_out: bfloat16 [4096, 2048], P(('ep', 'tp'))
Inputs may be any that keep to these rules, and one draw needn't show every extreme that they name: `selected_specialist_ids`: each row names 2 different experts. Among the rows of one device no expert is named more than 96 times, and in every draw some device names some expert exactly 96 times.
All inputs are finite; a program needn't handle non-finite values.
Results may differ from a plain program's by a relative error of at most 0.0085.
Values may be sent and summed in bfloat16 or wider, within the bound.
A program may use at most 128 MiB of HBM per device.

v0:
```python
import jax
import jax.numpy as jnp
from jax import lax
from jax.sharding import PartitionSpec as P

BLOCK = 64


def entering_2(x, axis, combine, identity):
    count, index = (lax.axis_size(axis), lax.axis_index(axis))
    everything = jax.tree.map(lambda part: lax.all_gather(part, axis), x)
    start = jax.tree.map(
        lambda part, zero: jnp.broadcast_to(jnp.asarray(zero, part.dtype), part.shape), x, identity
    )

    def hop(k, before):
        reached = k < index
        new = combine(before, jax.tree.map(lambda part: part[k], everything))
        return jax.tree.map(lambda a, b: jnp.where(reached, a, b), new, before)

    return lax.fori_loop(0, count, hop, start)


def from_behind(x, axis, by):
    count = lax.axis_size(axis)
    pairs = [(i, i + by) for i in range(count) if 0 <= i + by < count]
    return lax.ppermute(x, axis, pairs)


def combine_pairs(earlier, later):
    return (earlier[0] * later[0], later[0] * earlier[1] + later[1])


def expert_units(rows, gate_piece, up_piece):
    gate_pre = jnp.dot(rows, gate_piece, preferred_element_type=jnp.float32)
    up_pre = jnp.dot(rows, up_piece, preferred_element_type=jnp.float32)
    gate_cut = jnp.minimum(gate_pre, 7.0)
    up_cut = jnp.clip(up_pre, -7.0, 7.0)
    return ((up_cut + 1.0) * gate_cut * jax.nn.sigmoid(1.702 * gate_cut)).astype(jnp.bfloat16)


def down_product(units, down_piece):
    return lax.dot_general(
        units, down_piece, (((1,), (1,)), ((), ())), preferred_element_type=jnp.float32
    )


def segment_recurrence(decay, drive):
    channels, positions = decay.shape
    span = 16
    seg_count = positions // span
    decay_split = decay.reshape(channels, seg_count, span).transpose(0, 2, 1)
    drive_split = drive.reshape(channels, seg_count, span).transpose(0, 2, 1)
    run_state = jnp.zeros((channels, seg_count), jnp.float32)
    run_decay = jnp.ones((channels, seg_count), jnp.float32)
    state_list = []
    decay_list = []
    for offset in range(span):
        run_state = decay_split[:, offset] * run_state + drive_split[:, offset]
        run_decay = run_decay * decay_split[:, offset]
        state_list.append(run_state)
        decay_list.append(run_decay)
    local_state = jnp.stack(state_list, axis=1)
    local_decay = jnp.stack(decay_list, axis=1)
    decay_upto, state_upto = lax.associative_scan(combine_pairs, (run_decay, run_state), axis=1)
    decay_before = jnp.concatenate(
        [jnp.ones((channels, 1), jnp.float32), decay_upto[:, :-1]], axis=1
    )
    state_before = jnp.concatenate(
        [jnp.zeros((channels, 1), jnp.float32), state_upto[:, :-1]], axis=1
    )
    identity = (jnp.ones((channels,), jnp.float32), jnp.zeros((channels,), jnp.float32))
    carried = entering_2((decay_upto[:, -1], state_upto[:, -1]), "ep", combine_pairs, identity)
    entering = state_before + decay_before * carried[1][:, None]
    state = local_state + local_decay * entering[:, None, :]
    return state.transpose(0, 2, 1).reshape(channels, positions)


def mixer_half(
    scan_source_values,
    switch_path_values,
    causal_filter_coefficients,
    scan_switch_blockmap,
    entry_switch_blockmap,
    feature_fading_speeds,
    spike_amount,
    final_linear_map,
):
    channels, positions = scan_source_values.shape
    tp_index = lax.axis_index("tp")
    first_chan = tp_index * channels
    conv_local = lax.dynamic_slice_in_dim(
        causal_filter_coefficients, first_chan, channels, 0
    ).astype(jnp.float32)
    tap_count = conv_local.shape[1]
    rim_cells = from_behind(scan_source_values[:, positions - tap_count + 1 :], "ep", 1)
    padded = jnp.concatenate([rim_cells, scan_source_values], axis=1).astype(jnp.float32)
    running = padded[:, 0:positions] * conv_local[:, 0:1]
    for shift_tap in range(1, tap_count):
        running = (
            running
            + padded[:, shift_tap : shift_tap + positions]
            * conv_local[:, shift_tap : shift_tap + 1]
        )
    conv_out = running.astype(jnp.bfloat16)
    block_count = channels // BLOCK
    rate_local = lax.dynamic_slice_in_dim(
        scan_switch_blockmap, tp_index * block_count, block_count, 0
    )
    input_local = lax.dynamic_slice_in_dim(
        entry_switch_blockmap, tp_index * block_count, block_count, 0
    )
    grouped = conv_out.reshape(block_count, BLOCK, positions)
    block_dims = (((1,), (1,)), ((0,), (0,)))
    scan_switch = jax.nn.sigmoid(
        lax.dot_general(
            rate_local, grouped, block_dims, preferred_element_type=jnp.float32
        ).reshape(channels, positions)
    )
    inflow = jax.nn.sigmoid(
        lax.dot_general(
            input_local, grouped, block_dims, preferred_element_type=jnp.float32
        ).reshape(channels, positions)
    )
    feature_fading = lax.dynamic_slice_in_dim(feature_fading_speeds, first_chan, channels, 0)
    fading_exponent = -8.0 * scan_switch * feature_fading[:, None] + spike_amount[None, :]
    drive = jnp.sqrt(-jnp.expm1(2.0 * fading_exponent)) * inflow * conv_out.astype(jnp.float32)
    state = segment_recurrence(jnp.exp(fading_exponent), drive)
    mix_hidden = (
        state * jax.nn.gelu(switch_path_values.astype(jnp.float32), approximate=True)
    ).astype(jnp.bfloat16)
    tp_count = lax.axis_size("tp")
    pieces = mix_hidden.reshape(channels, tp_count, positions // tp_count)
    return lax.dot_general(
        lax.all_to_all(pieces, "tp", split_axis=1, concat_axis=0, tiled=True)[:, 0, :],
        final_linear_map,
        (((0,), (0,)), ((), ())),
        preferred_element_type=jnp.float32,
    ).astype(jnp.bfloat16)


def expert_half(
    dispatched_group_activity,
    specialist_rmsgain,
    selected_specialist_ids,
    selected_specialist_share,
    specialist_switch_maps,
    specialist_widen_maps,
    specialist_shrink_maps,
):
    token_count, model_width = dispatched_group_activity.shape
    route_count = selected_specialist_ids.shape[1]
    expert_count = lax.axis_size("ep")
    slot_count = 3 * route_count * token_count // (2 * expert_count)
    values = dispatched_group_activity.astype(jnp.float32)
    scale = lax.rsqrt(jnp.mean(values * values, axis=1, keepdims=True) + 1e-06)
    normed = (values * scale * specialist_rmsgain.astype(jnp.float32)).astype(jnp.bfloat16)
    flat_ids = selected_specialist_ids.reshape(-1)
    one_hot = (flat_ids[:, None] == jnp.arange(expert_count, dtype=jnp.int32)[None, :]).astype(
        jnp.int32
    )
    slot_rank = jnp.sum((jnp.cumsum(one_hot, axis=0) - one_hot) * one_hot, axis=1)
    slot_place = flat_ids * slot_count + slot_rank
    owner_token = jnp.arange(token_count * route_count, dtype=jnp.int32) // route_count
    slot_token = (
        jnp.full((expert_count * slot_count,), token_count, jnp.int32)
        .at[slot_place]
        .set(owner_token)
    )
    padded_rows = jnp.concatenate([normed, jnp.zeros((1, model_width), jnp.bfloat16)], axis=0)
    outgoing = padded_rows[slot_token].reshape(expert_count, slot_count, model_width)
    arrived = lax.all_to_all(outgoing, "ep", split_axis=0, concat_axis=0, tiled=True).reshape(
        expert_count * slot_count, model_width
    )
    gate_shard = specialist_switch_maps[0]
    up_shard = specialist_widen_maps[0]
    down_shard = specialist_shrink_maps[0]
    result = down_product(
        expert_units(
            arrived,
            lax.all_gather(gate_shard, "tp", axis=1, tiled=True),
            lax.all_gather(up_shard, "tp", axis=1, tiled=True),
        ),
        lax.all_gather(down_shard, "tp", axis=1, tiled=True),
    )
    outbound = result.astype(jnp.bfloat16).reshape(expert_count, slot_count, model_width)
    returned = lax.all_to_all(outbound, "ep", split_axis=0, concat_axis=0, tiled=True).reshape(
        expert_count * slot_count, model_width
    )
    chosen = returned[slot_place].reshape(token_count, route_count, model_width).astype(jnp.float32)
    return jnp.sum(chosen * selected_specialist_share[:, :, None], axis=1).astype(jnp.bfloat16)


def on_device(
    scan_source_values,
    switch_path_values,
    causal_filter_coefficients,
    scan_switch_blockmap,
    entry_switch_blockmap,
    feature_fading_speeds,
    spike_amount,
    final_linear_map,
    dispatched_group_activity,
    specialist_rmsgain,
    selected_specialist_ids,
    selected_specialist_share,
    specialist_switch_maps,
    specialist_widen_maps,
    specialist_shrink_maps,
):
    scan_path_result = mixer_half(
        scan_source_values,
        switch_path_values,
        causal_filter_coefficients,
        scan_switch_blockmap,
        entry_switch_blockmap,
        feature_fading_speeds,
        spike_amount,
        final_linear_map,
    )
    moe_out = expert_half(
        dispatched_group_activity,
        specialist_rmsgain,
        selected_specialist_ids,
        selected_specialist_share,
        specialist_switch_maps,
        specialist_widen_maps,
        specialist_shrink_maps,
    )
    return (scan_path_result, moe_out)


def solution(mesh):
    in_specs = (
        P("tp", "ep"),
        P("tp", "ep"),
        P(),
        P(),
        P(),
        P(),
        P("ep"),
        P(),
        P(("ep", "tp"), None),
        P(),
        P(("ep", "tp"), None),
        P(("ep", "tp"), None),
        P("ep", None, "tp"),
        P("ep", None, "tp"),
        P("ep", None, "tp"),
    )
    out_specs = (P(("ep", "tp"), None), P(("ep", "tp"), None))
    return jax.shard_map(
        on_device, mesh=mesh, in_specs=in_specs, out_specs=out_specs, check_vma=False
    )
```

profile of v0, /device:TPU:0, one launch (start us, length us, event | category | flops | bytes accessed | tf_op | source)
XLA Modules:
  0.0 313.0 jit_solution(17544688846019804012)
XLA Ops:
  9.5 4.9 %collective-permute-start = (bf16[128,3]{1,0:T(8,128)(2,1)S(1)}, bf16[128,3]{1,0:T(8,128)(2,1)S(1)}, u32[]{:S(2)}, u32[]{:S(2)}) collective-permute-start(bf16[128,3]{1,0:T(8,128)(2,1)S(1)} %slice.357), channel_id=1, source_target_pairs={{0,8},{8,16},{16,24},{1,9},{9,17},{17,25},{2,10},{10,18},{18,26},{... | collective-permute-start | bytes 2312 | tf_op jit(solution)/shard_map/ppermute | solution.py:27
  18.7 3.1 gather_fusion
  21.8 4.7 %all-to-all-start.1 = ((bf16[4,96,2048]{2,1,0:T(8,128)(2,1)}), bf16[4,96,2048]{2,1,0:T(8,128)(2,1)}, u32[]{:S(2)}, u32[]{:S(2)}) async-start(bf16[4,96,2048]{2,1,0:T(8,128)(2,1)} %bitcast.90), calls=%async_computation.1 | async-start | bytes 3145728 | tf_op jit(solution)/shard_map/all_to_all | solution.py:172
  29.9 1.8 fusion.30
  31.8 2.5 fusion.16
  34.3 2.7 copy.112
  37.0 2.1 div.32
  39.1 1.6 exponential_bitcast_fusion
  44.8 1.6 fusion.13
  46.4 1.9 fusion.33
  58.6 2.5 stack.5
  61.1 3.2 %stack.4 = f32[128,16,128]{0,1,2:T(8,128)S(1)} concatenate(f32[128,1,128]{0,1,2:T(1,128)} %bitcast.369, f32[128,1,128]{0,1,2:T(1,128)} %bitcast.368, f32[128,1,128]{0,1,2:T(1,128)} %bitcast.367, f32[128,1,128]{0,1,2:T(1,128)} %bitcast.366, f32[128,1,128]{0,1,2:T(1,128)S(1)} %bitcast.365, f32[128,1,128]{0,1,2:T(1,128)S(1)} %bitcast.364, f32[128,1,128]{0,1,2:T(1,128)S(1)} %bitcast.363, ...), dimensions={1} | concatenate | bytes 2097152 | tf_op jit(solution)/shard_map/stack | solution.py:63
  64.3 8.2 %all-gather.1 = f32[512,1]{0,1:T(1,128)S(1)} all-gather(f32[128,1]{0,1:T(1,128)S(1)} %slice.620), channel_id=3, replica_groups=mesh['ep'=4,'tp'=8] {'ep'}, dimensions={0}, use_global_device_ids=true | all-gather | bytes 2560 | tf_op jit(solution)/shard_map/all_gather | solution.py:11
  72.5 7.9 %all-gather = f32[512,1]{0,1:T(1,128)S(1)} all-gather(f32[128,1]{0,1:T(1,128)S(1)} %slice.618), channel_id=2, replica_groups=mesh['ep'=4,'tp'=8] {'ep'}, dimensions={0}, use_global_device_ids=true | all-gather | bytes 2560 | tf_op jit(solution)/shard_map/all_gather | solution.py:11
  83.9 4.9 %all-to-all-start = ((bf16[128,8,256]{2,0,1:T(8,128)(2,1)}), bf16[128,8,256]{2,0,1:T(8,128)(2,1)S(1)}, u32[]{:S(2)}, u32[]{:S(2)}) async-start(bf16[128,8,256]{2,0,1:T(8,128)(2,1)} %copy.169), calls=%async_computation | async-start | bytes 1048576 | tf_op jit(solution)/shard_map/all_to_all | solution.py:135
  88.8 6.2 %all-gather.11.cloned.1.call-done = bf16[1,2048,2048]{2,1,0:T(8,128)(2,1)} async-done(((bf16[1,2048,256]{2,1,0:T(8,128)(2,1)}), bf16[1,2048,2048]{2,1,0:T(8,128)(2,1)}) %all-gather.11.cloned.1.call-update) | async-done | bytes 8388624 | tf_op jit(solution)/shard_map/all_gather | solution.py:181
  95.0 8.9 %fusion.2 = f32[384,2048]{1,0:T(8,128)} fusion(bf16[384,2048]{1,0:T(8,128)(2,1)} %bitcast.91, bf16[1,2048,2048]{2,1,0:T(8,128)(2,1)} %all-gather.11.cloned.1.call-done), kind=kOutput, calls=%fused_computation.9 | convolution fusion | flops 3221225472 | bytes 13107200 | tf_op jit(solution)/shard_map/dot_general | solution.py:35
  103.9 74.5 %all-gather.13.cloned.1.call-done = bf16[1,2048,2048]{2,1,0:T(8,128)(2,1)} async-done(((bf16[1,2048,256]{2,1,0:T(8,128)(2,1)}), bf16[1,2048,2048]{2,1,0:T(8,128)(2,1)}) %all-gather.13.cloned.1.call-update) | async-done | bytes 8388624 | tf_op jit(solution)/shard_map/all_gather | solution.py:184
  178.4 82.3 %all-gather.9.cloned.1.call-done = bf16[1,2048,2048]{2,1,0:T(8,128)(2,1)} async-done(((bf16[1,2048,256]{2,1,0:T(8,128)(2,1)}), bf16[1,2048,2048]{2,1,0:T(8,128)(2,1)}) %all-gather.9.cloned.1.call-update) | async-done | bytes 8388624 | tf_op jit(solution)/shard_map/all_gather | solution.py:182
  260.7 15.6 %fusion.8 = bf16[384,2048]{1,0:T(8,128)(2,1)} fusion(bf16[1,2048,2048]{2,1,0:T(8,128)(2,1)} %all-gather.13.cloned.1.call-done, f32[384,2048]{1,0:T(8,128)} %fusion.2, bf16[384,2048]{1,0:T(8,128)(2,1)} %bitcast.91, bf16[1,2048,2048]{2,1,0:T(8,128)(2,1)} %all-gather.9.cloned.1.call-done), kind=kOutput, calls=%fused_computation.14 | convolution fusion | flops 6451101696 | bytes 23068672 | tf_op jit(solution)/shard_map/dot_general | solution.py:43
  276.4 3.8 %all-to-all-start.2 = ((bf16[4,96,2048]{2,1,0:T(8,128)(2,1)}), bf16[4,96,2048]{2,1,0:T(8,128)(2,1)S(1)}, u32[]{:S(2)}, u32[]{:S(2)}) async-start(bf16[4,96,2048]{2,1,0:T(8,128)(2,1)} %bitcast.95), calls=%async_computation.2 | async-start | bytes 3145728 | tf_op jit(solution)/shard_map/all_to_all | solution.py:187
  280.3 4.4 %convolution_convert_fusion = bf16[256,2048]{1,0:T(8,128)(2,1)} fusion(bf16[1024,256]{1,0:T(8,128)(2,1)S(1)} %bitcast.354, bf16[1024,2048]{1,0:T(8,128)(2,1)} %param.24), kind=kOutput, calls=%fused_computation.15 | convolution fusion | flops 1074266112 | bytes 5767168 | tf_op jit(solution)/shard_map/dot_general | solution.py:134
  284.8 15.1 %all-to-all-done.2 = bf16[4,96,2048]{2,1,0:T(8,128)(2,1)S(1)} async-done(((bf16[4,96,2048]{2,1,0:T(8,128)(2,1)}), bf16[4,96,2048]{2,1,0:T(8,128)(2,1)S(1)}, u32[]{:S(2)}, u32[]{:S(2)}) %all-to-all-start.2) | async-done | bytes 1572896 | tf_op jit(solution)/shard_map/all_to_all | solution.py:187
  302.6 3.9 %multiply_reduce_fusion = bf16[128,2048]{1,0:T(8,128)(2,1)} fusion(f32[128,2,2048]{2,1,0:T(2,128)S(1)} %reshape.132, f32[128,2]{1,0:T(8,128)S(1)} %copy.175), kind=kLoop, calls=%fused_computation.24 | loop fusion | flops 786432 | bytes 2622464 | tf_op jit(solution)/shard_map/reduce_sum | solution.py:191
  (283 shorter events, 29.8 us)
Async XLA Ops:
  7.2 24.6 %copy-start = (bf16[16,64,64]{2,1,0:T(8,128)(2,1)S(1)}, bf16[16,64,64]{2,1,0:T(8,128)(2,1)}, u32[]{:S(2)}) copy-start(bf16[16,64,64]{2,1,0:T(8,128)(2,1)} %param.20) | copy-start | bytes 393220
  7.2 7.2 %copy-start.48 = (s32[128,2]{0,1:T(2,128)S(1)}, s32[128,2]{0,1:T(2,128)}, u32[]{:S(2)}) copy-start(s32[128,2]{0,1:T(2,128)} %param.27) | copy-start | bytes 3076
  7.2 9.4 %copy-start.49 = (bf16[2048]{0:T(1024)(128)(2,1)S(1)}, bf16[2048]{0:T(1024)(128)(2,1)}, u32[]{:S(2)}) copy-start(bf16[2048]{0:T(1024)(128)(2,1)} %param.26) | copy-start | bytes 12292
  7.2 9.4 %copy-start.3 = (bf16[128,2048]{1,0:T(8,128)(2,1)S(1)}, bf16[128,2048]{1,0:T(8,128)(2,1)}, u32[]{:S(2)}) copy-start(bf16[128,2048]{1,0:T(8,128)(2,1)} %param.25) | copy-start | bytes 1572868
  7.2 87.7 %all-gather.11.cloned.1.call-start = ((), (), s32[]{:S(2)}) async-start(), calls=%async_computation.4 | async-start | bytes 9437184 | tf_op jit(solution)/shard_map/all_gather | solution.py:181
  8.0 170.4 %all-gather.13.cloned.1.call-start = ((), (), s32[]{:S(2)}) async-start(), calls=%async_computation.5 | async-start | bytes 9437184 | tf_op jit(solution)/shard_map/all_gather | solution.py:184
  8.7 252.0 %all-gather.9.cloned.1.call-start = ((), (), s32[]{:S(2)}) async-start(), calls=%async_computation.3 | async-start | bytes 9437184 | tf_op jit(solution)/shard_map/all_gather | solution.py:182
  9.5 20.2 %collective-permute-start = (bf16[128,3]{1,0:T(8,128)(2,1)S(1)}, bf16[128,3]{1,0:T(8,128)(2,1)S(1)}, u32[]{:S(2)}, u32[]{:S(2)}) collective-permute-start(bf16[128,3]{1,0:T(8,128)(2,1)S(1)} %slice.357), channel_id=1, source_target_pairs={{0,8},{8,16},{16,24},{1,9},{9,17},{17,25},{2,10},{10,18},{18,26},{... | collective-permute-start | bytes 2312 | tf_op jit(solution)/shard_map/ppermute | solution.py:27
  21.8 62.1 %all-to-all-start.1 = ((bf16[4,96,2048]{2,1,0:T(8,128)(2,1)}), bf16[4,96,2048]{2,1,0:T(8,128)(2,1)}, u32[]{:S(2)}, u32[]{:S(2)}) async-start(bf16[4,96,2048]{2,1,0:T(8,128)(2,1)} %bitcast.90), calls=%async_computation.1 | async-start | bytes 3145728 | tf_op jit(solution)/shard_map/all_to_all | solution.py:172
  50.4 8.2 %copy-start.29 = (f32[128,1,128]{0,2,1:T(8,128)S(1)}, f32[128,1,128]{0,2,1:T(8,128)}, u32[]{:S(2)}) copy-start(f32[128,1,128]{0,2,1:T(8,128)} %copy-done.28) | copy-start | bytes 196612
  50.4 8.2 %copy-start.36 = (f32[128,1,128]{0,1,2:T(1,128)S(1)}, f32[128,1,128]{0,1,2:T(1,128)}, u32[]{:S(2)}) copy-start(f32[128,1,128]{0,1,2:T(1,128)} %get-tuple-element.157) | copy-start | bytes 196612
  50.4 8.2 %copy-start.37 = (f32[128,1,128]{0,2,1:T(8,128)S(1)}, f32[128,1,128]{0,2,1:T(8,128)}, u32[]{:S(2)}) copy-start(f32[128,1,128]{0,2,1:T(8,128)} %get-tuple-element.126) | copy-start | bytes 196612
  50.4 8.2 %copy-start.38 = (f32[128,1,128]{0,2,1:T(8,128)S(1)}, f32[128,1,128]{0,2,1:T(8,128)}, u32[]{:S(2)}) copy-start(f32[128,1,128]{0,2,1:T(8,128)} %get-tuple-element.127) | copy-start | bytes 196612
  50.4 8.2 %copy-start.39 = (f32[128,1,128]{0,2,1:T(8,128)S(1)}, f32[128,1,128]{0,2,1:T(8,128)}, u32[]{:S(2)}) copy-start(f32[128,1,128]{0,2,1:T(8,128)} %get-tuple-element.128) | copy-start | bytes 196612
  50.4 8.2 %copy-start.40 = (f32[128,1,128]{0,2,1:T(8,128)S(1)}, f32[128,1,128]{0,2,1:T(8,128)}, u32[]{:S(2)}) copy-start(f32[128,1,128]{0,2,1:T(8,128)} %get-tuple-element.129) | copy-start | bytes 196612
  50.4 8.2 %copy-start.41 = (f32[128,1,128]{0,2,1:T(8,128)S(1)}, f32[128,1,128]{0,2,1:T(8,128)}, u32[]{:S(2)}) copy-start(f32[128,1,128]{0,2,1:T(8,128)} %get-tuple-element.130) | copy-start | bytes 196612
  50.4 8.2 %copy-start.42 = (f32[128,1,128]{0,2,1:T(8,128)S(1)}, f32[128,1,128]{0,2,1:T(8,128)}, u32[]{:S(2)}) copy-start(f32[128,1,128]{0,2,1:T(8,128)} %get-tuple-element.131) | copy-start | bytes 196612
  50.4 8.2 %copy-start.43 = (f32[128,1,128]{0,2,1:T(8,128)S(1)}, f32[128,1,128]{0,2,1:T(8,128)}, u32[]{:S(2)}) copy-start(f32[128,1,128]{0,2,1:T(8,128)} %get-tuple-element.132) | copy-start | bytes 196612
  51.3 9.8 %copy-start.33 = (f32[128,1,128]{0,2,1:T(8,128)S(1)}, f32[128,1,128]{0,2,1:T(8,128)}, u32[]{:S(2)}) copy-start(f32[128,1,128]{0,2,1:T(8,128)} %get-tuple-element.149) | copy-start | bytes 196612
  51.3 9.8 %copy-start.34 = (f32[128,1,128]{0,2,1:T(8,128)S(1)}, f32[128,1,128]{0,2,1:T(8,128)}, u32[]{:S(2)}) copy-start(f32[128,1,128]{0,2,1:T(8,128)} %get-tuple-element.150) | copy-start | bytes 196612
  56.0 24.4 %copy-start.35 = (f32[128,128]{0,1:T(8,128)S(1)}, f32[128,128]{0,1:T(8,128)}, u32[]{:S(2)}) copy-start(f32[128,128]{0,1:T(8,128)} %pad.102) | copy-start | bytes 196612
  61.1 21.4 %copy-start.4 = (bf16[128,2048]{0,1:T(8,128)(2,1)S(1)}, bf16[128,2048]{0,1:T(8,128)(2,1)}, u32[]{:S(2)}) copy-start(bf16[128,2048]{0,1:T(8,128)(2,1)} %copy.168) | copy-start | bytes 1572868
  83.9 192.5 %all-to-all-start = ((bf16[128,8,256]{2,0,1:T(8,128)(2,1)}), bf16[128,8,256]{2,0,1:T(8,128)(2,1)S(1)}, u32[]{:S(2)}, u32[]{:S(2)}) async-start(bf16[128,8,256]{2,0,1:T(8,128)(2,1)} %copy.169), calls=%async_computation | async-start | bytes 1048576 | tf_op jit(solution)/shard_map/all_to_all | solution.py:135
  276.4 23.5 %all-to-all-start.2 = ((bf16[4,96,2048]{2,1,0:T(8,128)(2,1)}), bf16[4,96,2048]{2,1,0:T(8,128)(2,1)S(1)}, u32[]{:S(2)}, u32[]{:S(2)}) async-start(bf16[4,96,2048]{2,1,0:T(8,128)(2,1)} %bitcast.95), calls=%async_computation.2 | async-start | bytes 3145728 | tf_op jit(solution)/shard_map/all_to_all | solution.py:187
  (38 other events, 110.9 us)
Sparse Core Ops, SparseCore 0:
  9.6 85.2 all-gather.10
  96.5 81.8 all-gather.12
  180.0 80.6 all-gather.8
where the time goes:
time: 314 us; the launch traced here: 313 us
  waiting for transfers between devices  180 us (57%)
  matrix products  33.1 us (11%)
  local copies, waits for them, and re-layouts  30.1 us (10%)
  other arithmetic  20.2 us (6%)
  starting transfers between devices  18.4 us (6%)
  blocking collectives  16 us (5%)
  between operations  15 us (5%)
    all_gather x1, waiting for transfers between devices, expert_half(): lax.all_gather(up_shard, 'tp', axis=1, tiled=True)  82.3 us
    all_gather x1, waiting for transfers between devices, expert_half(): lax.all_gather(down_shard, 'tp', axis=1, tiled=True)  74.5 us
    all_gather x2, blocking collectives, entering_2(): everything = jax.tree.map(lambda part: lax.all_gather(part, axis), x)  16 us
    dot_general x1, matrix products, down_product(): lax.dot_general(units, down_piece, (((1,), (1,)), ((), ())), preferred_el...  15.6 us
    all_to_all x1, waiting for transfers between devices, expert_half(): lax.all_to_all(outbound, 'ep', split_axis=0, concat_axis=0, tiled=True)  15.1 us
    dot_general x1, matrix products, expert_units(): gate_pre = jnp.dot(rows, gate_piece, preferred_element_type=jnp.float32)  8.92 us
  transfers between devices with their start and end apart: 7, of which 4 were waited for; matrix products, arithmetic and copies ran while one was open for 24% of the time, Pallas kernels for 0%

commit v1 on v0

--- a/solution.py
+++ b/solution.py
@@ -8,17 +8,13 @@
 
 def entering_2(x, axis, combine, identity):
     count, index = (lax.axis_size(axis), lax.axis_index(axis))
-    everything = jax.tree.map(lambda part: lax.all_gather(part, axis), x)
-    start = jax.tree.map(
-        lambda part, zero: jnp.broadcast_to(jnp.asarray(zero, part.dtype), part.shape), x, identity
-    )
-
-    def hop(k, before):
+    packed = lax.all_gather(jnp.stack(x), axis)
+    before = identity
+    for k in range(count):
+        new = combine(before, (packed[k, 0], packed[k, 1]))
         reached = k < index
-        new = combine(before, jax.tree.map(lambda part: part[k], everything))
-        return jax.tree.map(lambda a, b: jnp.where(reached, a, b), new, before)
-
-    return lax.fori_loop(0, count, hop, start)
+        before = jax.tree.map(lambda a, b: jnp.where(reached, a, b), new, before)
+    return before
 
 
 def from_behind(x, axis, by):
@@ -139,6 +135,51 @@
     ).astype(jnp.bfloat16)
 
 
+def slot_places(ids, expert_count, slot_count):
+    token_count = ids.shape[0]
+    experts = jnp.arange(expert_count, dtype=jnp.int32)[None, None, :]
+    named = (ids[:, :, None] == experts).astype(jnp.bfloat16)
+    member = jnp.sum(named.astype(jnp.float32), axis=1).astype(jnp.bfloat16)
+    order = jnp.arange(token_count, dtype=jnp.int32)
+    earlier = (order[None, :] < order[:, None]).astype(jnp.bfloat16)
+    rank = jnp.dot(earlier, member, preferred_element_type=jnp.float32)
+    own_rank = jnp.sum(named.astype(jnp.float32) * rank[:, None, :], axis=2).astype(jnp.int32)
+    return ids * slot_count + own_rank
+
+
+def normed_rows(activity, gain):
+    values = activity.astype(jnp.float32)
+    scale = lax.rsqrt(jnp.mean(values * values, axis=1, keepdims=True) + 1e-06)
+    return (values * scale * gain.astype(jnp.float32)).astype(jnp.bfloat16)
+
+
+def rows_in_slots(rows, places, slot_total):
+    slots = jnp.arange(slot_total, dtype=jnp.int32)[:, None]
+    picks = slots == places[:, 0][None, :]
+    for route in range(1, places.shape[1]):
+        picks = picks | (slots == places[:, route][None, :])
+    return jnp.dot(
+        picks.astype(jnp.bfloat16), rows, preferred_element_type=jnp.float32
+    ).astype(jnp.bfloat16)
+
+
+def weighted_routes(returned, places, share):
+    slots = jnp.arange(returned.shape[0], dtype=jnp.int32)[None, :]
+    total = None
+    for route in range(places.shape[1]):
+        picks = (slots == places[:, route][:, None]).astype(jnp.bfloat16)
+        chosen = jnp.dot(picks, returned, preferred_element_type=jnp.float32)
+        term = chosen * share[:, route][:, None]
+        total = term if total is None else total + term
+    return total
+
+
+def over_experts(rows, expert_count):
+    width = rows.shape[1]
+    pieces = rows.reshape(expert_count, rows.shape[0] // expert_count, width)
+    return lax.all_to_all(pieces, "ep", split_axis=0, concat_axis=0, tiled=True).reshape(-1, width)
+
+
 def expert_half(
     dispatched_group_activity,
     specialist_rmsgain,
@@ -152,43 +193,46 @@
     route_count = selected_specialist_ids.shape[1]
     expert_count = lax.axis_size("ep")
     slot_count = 3 * route_count * token_count // (2 * expert_count)
-    values = dispatched_group_activity.astype(jnp.float32)
-    scale = lax.rsqrt(jnp.mean(values * values, axis=1, keepdims=True) + 1e-06)
-    normed = (values * scale * specialist_rmsgain.astype(jnp.float32)).astype(jnp.bfloat16)
-    flat_ids = selected_specialist_ids.reshape(-1)
-    one_hot = (flat_ids[:, None] == jnp.arange(expert_count, dtype=jnp.int32)[None, :]).astype(
-        jnp.int32
-    )
-    slot_rank = jnp.sum((jnp.cumsum(one_hot, axis=0) - one_hot) * one_hot, axis=1)
-    slot_place = flat_ids * slot_count + slot_rank
-    owner_token = jnp.arange(token_count * route_count, dtype=jnp.int32) // route_count
-    slot_token = (
-        jnp.full((expert_count * slot_count,), token_count, jnp.int32)
-        .at[slot_place]
-        .set(owner_token)
-    )
-    padded_rows = jnp.concatenate([normed, jnp.zeros((1, model_width), jnp.bfloat16)], axis=0)
-    outgoing = padded_rows[slot_token].reshape(expert_count, slot_count, model_width)
-    arrived = lax.all_to_all(outgoing, "ep", split_axis=0, concat_axis=0, tiled=True).reshape(
-        expert_count * slot_count, model_width
-    )
-    gate_shard = specialist_switch_maps[0]
-    up_shard = specialist_widen_maps[0]
-    down_shard = specialist_shrink_maps[0]
-    result = down_product(
-        expert_units(
-            arrived,
-            lax.all_gather(gate_shard, "tp", axis=1, tiled=True),
-            lax.all_gather(up_shard, "tp", axis=1, tiled=True),
-        ),
-        lax.all_gather(down_shard, "tp", axis=1, tiled=True),
-    )
-    outbound = result.astype(jnp.bfloat16).reshape(expert_count, slot_count, model_width)
-    returned = lax.all_to_all(outbound, "ep", split_axis=0, concat_axis=0, tiled=True).reshape(
-        expert_count * slot_count, model_width
-    )
-    chosen = returned[slot_place].reshape(token_count, route_count, model_width).astype(jnp.float32)
-    return jnp.sum(chosen * selected_specialist_share[:, :, None], axis=1).astype(jnp.bfloat16)
+    slot_total = expert_count * slot_count
+    tp_count = lax.axis_size("tp")
+    half = tp_count // 2
+    swap = [(i, (i + half) % tp_count) for i in range(tp_count)]
+    halves = [list(range(half)), list(range(half, tp_count))]
+
+    def gather_half(piece):
+        return lax.all_gather(piece, "tp", axis=1, tiled=True, axis_index_groups=halves)
+
+    table = jnp.concatenate(
+        [selected_specialist_ids.astype(jnp.float32), selected_specialist_share], axis=1
+    )
+    far_table = lax.ppermute(table, "tp", swap)
+    far_activity = lax.ppermute(dispatched_group_activity, "tp", swap)
+    gate_full = gather_half(specialist_switch_maps[0])
+    up_full = gather_half(specialist_widen_maps[0])
+    down_full = gather_half(specialist_shrink_maps[0])
+
+    near_places = slot_places(selected_specialist_ids, expert_count, slot_count)
+    near_rows = rows_in_slots(
+        normed_rows(dispatched_group_activity, specialist_rmsgain), near_places, slot_total
+    )
+    near_arrived = over_experts(near_rows, expert_count)
+    far_ids = far_table[:, :route_count].astype(jnp.int32)
+    far_share = far_table[:, route_count:]
+    far_places = slot_places(far_ids, expert_count, slot_count)
+    far_rows = rows_in_slots(
+        normed_rows(far_activity, specialist_rmsgain), far_places, slot_total
+    )
+    far_arrived = over_experts(far_rows, expert_count)
+    arrived = jnp.concatenate([far_arrived, near_arrived], axis=0)
+    units = expert_units(arrived, gate_full, up_full)
+    far_result = down_product(units[:slot_total], down_full).astype(jnp.bfloat16)
+    far_returned = over_experts(far_result, expert_count)
+    near_result = down_product(units[slot_total:], down_full).astype(jnp.bfloat16)
+    near_returned = over_experts(near_result, expert_count)
+    far_sum = weighted_routes(far_returned, far_places, far_share).astype(jnp.bfloat16)
+    home_sum = lax.ppermute(far_sum, "tp", swap)
+    near_sum = weighted_routes(near_returned, near_places, selected_specialist_share)
+    return (near_sum + home_sum.astype(jnp.float32)).astype(jnp.bfloat16)
 
 
 def on_device(

time: 314 us -> 241 us (0.77)
  waiting for transfers between devices: 180 us -> 94.5 us
  starting transfers between devices: 18.4 us -> 30.6 us
  matrix products: 33.1 us -> 44 us
  local copies, waits for them, and re-layouts: 30.1 us -> 21 us
  blocking collectives: 16 us -> 8.54 us
  other arithmetic: 20.2 us -> 25.7 us
    all_gather x3, waiting for transfers between devices: 163 us -> 44.7 us  [gather_half(): lax.all_gather(piece, 'tp', axis=1, tiled=True, axis_index_groups=halves)]
    all_to_all x2 -> x4, waiting for transfers between devices: 15.1 us -> 35.1 us  [over_experts(): lax.all_to_all(pieces, 'ep', split_axis=0, concat_axis=0, tiled=True)]
    dot_general x0 -> x9, matrix products: none -> 17.7 us  [the longest x1 8.86 us: expert_units(): up_pre = jnp.dot(rows, up_piece, preferred_element_type=jnp.float32)]
    ppermute x0 -> x3, waiting for transfers between devices: none -> 12.7 us  [the longest x1 12.7 us: expert_half(): home_sum = lax.ppermute(far_sum, 'tp', swap)]
    all_gather x2 -> x1, blocking collectives: 16 us -> 8.54 us  [entering_2(): packed = lax.all_gather(jnp.stack(x), axis)]
    all_to_all x2 -> x4, starting transfers between devices: 8.53 us -> 15.7 us  [over_experts(): lax.all_to_all(pieces, 'ep', split_axis=0, concat_axis=0, tiled=True)]
    another operation x4 -> x0, local copies, waits for them, and re-layouts: 5.74 us -> none  [the longest x1 3.19 us: segment_recurrence(): local_state = jnp.stack(state_list, axis=1)]
    ppermute x0 -> x3, starting transfers between devices: none -> 5.34 us  [the longest x1 2.59 us: expert_half(): far_table = lax.ppermute(table, 'tp', swap)]
  transfers between devices with their start and end apart: 7 -> 12, of which waited for: 4 -> 6; matrix products, arithmetic and copies ran while one was open for 24% -> 37% of each run, Pallas kernels for 0% -> 0%
where the time goes in v1:
time: 241 us; the launch traced here: 240 us
  waiting for transfers between devices  94.5 us (39%)
  matrix products  44 us (18%)
  starting transfers between devices  30.6 us (13%)
  other arithmetic  25.7 us (11%)
  local copies, waits for them, and re-layouts  21 us (9%)
  between operations  15.3 us (6%)
  blocking collectives  8.54 us (4%)
    all_gather x3, waiting for transfers between devices, gather_half(): lax.all_gather(piece, 'tp', axis=1, tiled=True, axis_index_groups=halves)  44.7 us
    all_to_all x4, waiting for transfers between devices, over_experts(): lax.all_to_all(pieces, 'ep', split_axis=0, concat_axis=0, tiled=True)  35.1 us
    all_to_all x4, starting transfers between devices, over_experts(): lax.all_to_all(pieces, 'ep', split_axis=0, concat_axis=0, tiled=True)  15.7 us
    ppermute x1, waiting for transfers between devices, expert_half(): home_sum = lax.ppermute(far_sum, 'tp', swap)  12.7 us
    dot_general x2, matrix products, down_product(): lax.dot_general(units, down_piece, (((1,), (1,)), ((), ())), preferred_el...  10.9 us
    dot_general x1, matrix products, expert_units(): up_pre = jnp.dot(rows, up_piece, preferred_element_type=jnp.float32)  8.86 us
    all_gather x1, blocking collectives, entering_2(): packed = lax.all_gather(jnp.stack(x), axis)  8.54 us
    dot_general x1, matrix products, expert_units(): gate_pre = jnp.dot(rows, gate_piece, preferred_element_type=jnp.float32)  7.75 us
  transfers between devices with their start and end apart: 12, of which 6 were waited for; matrix products, arithmetic and copies ran while one was open for 37% of the time, Pallas kernels for 0%

profile of v1, /device:TPU:0, one launch (start us, length us, event | category | flops | bytes accessed | tf_op | source)
XLA Modules:
  0.0 239.6 jit_solution(18344930823871556606)
XLA Ops:
  9.5 4.9 %collective-permute-start = (bf16[128,3]{1,0:T(8,128)(2,1)S(1)}, bf16[128,3]{1,0:T(8,128)(2,1)S(1)}, u32[]{:S(2)}, u32[]{:S(2)}) collective-permute-start(bf16[128,3]{1,0:T(8,128)(2,1)S(1)} %slice.415), channel_id=1, source_target_pairs={{0,8},{8,16},{16,24},{1,9},{9,17},{17,25},{2,10},{10,18},{18,26},{... | collective-permute-start | bytes 2312 | tf_op jit(solution)/shard_map/ppermute | solution.py:23
  17.9 2.6 %collective-permute-start.1 = (f32[128,4]{0,1:T(4,128)}, f32[128,4]{0,1:T(4,128)}, u32[]{:S(2)}, u32[]{:S(2)}) collective-permute-start(f32[128,4]{0,1:T(4,128)} %pad_maximum_fusion.15), channel_id=1, source_target_pairs={{0,4},{1,5},{2,6},{3,7},{4,0},{5,1},{6,2},{7,3},{8,12},{9,13},{10,... | collective-permute-start | bytes 6152 | tf_op jit(solution)/shard_map/ppermute | solution.py:208
  22.8 2.9 %convolution_convert_fusion = bf16[384,2048]{1,0:T(8,128)(2,1)} fusion(bf16[128,2048]{1,0:T(8,128)(2,1)} %param.23, f32[128]{0:T(128)S(1)} %add_rsqrt_fusion, f32[2048]{0:T(1024)S(1)} %convert_element_type.113, s32[128]{0:T(128)S(1)} %get-tuple-element.109, s32[128]{0:T(128)S(1)} %get-tuple-element.108), kind=kOutput, calls=%fused_computation.12 | convolution fusion | flops 203309056 | bytes 2106880 | tf_op jit(solution)/shard_map/dot_general | solution.py:161
  25.7 4.5 %all-to-all-start.2 = ((bf16[4,96,2048]{2,1,0:T(8,128)(2,1)}), bf16[4,96,2048]{2,1,0:T(8,128)(2,1)}, u32[]{:S(2)}, u32[]{:S(2)}) async-start(bf16[4,96,2048]{2,1,0:T(8,128)(2,1)} %bitcast.66), calls=%async_computation.2 | async-start | bytes 3145728 | tf_op jit(solution)/shard_map/all_to_all | solution.py:180
  37.6 2.7 %copy.119 = f32[2,64,2048]{1,0,2:T(2,128)S(1)} copy(f32[2,64,2048]{2,1,0:T(8,128)} %fusion.20) | data formatting | bytes 2097152 | tf_op jit(solution)/shard_map/div | solution.py:111
  40.3 2.1 div.26
  63.5 8.5 %all-gather.4 = f32[4,2,128]{2,1,0:T(2,128)S(1)} all-gather(f32[1,2,128]{2,1,0:T(2,128)S(1)} %maximum_bitcast_fusion), channel_id=2, replica_groups=mesh['ep'=4,'tp'=8] {'ep'}, dimensions={0}, use_global_device_ids=true | all-gather | bytes 5120 | tf_op jit(solution)/shard_map/all_gather | solution.py:11
  76.6 2.9 %convolution_convert_fusion.1 = bf16[384,2048]{1,0:T(8,128)(2,1)} fusion(bf16[128,2048]{1,0:T(8,128)(2,1)} %collective-permute-done.2, f32[2048]{0:T(1024)S(1)} %convert_element_type.113, f32[128]{0:T(128)S(1)} %add_rsqrt_fusion.1, s32[128]{0:T(128)S(1)} %get-tuple-element.105, s32[128]{0:T(128)S(1)} %get-tuple-element.104), kind=kOutput, calls=%fused_computation.13 | convolution fusion | flops 203309056 | bytes 2106880 | tf_op jit(solution)/shard_map/dot_general | solution.py:161
  79.5 3.8 %all-to-all-start.1 = ((bf16[4,96,2048]{2,1,0:T(8,128)(2,1)}), bf16[4,96,2048]{2,1,0:T(8,128)(2,1)S(1)}, u32[]{:S(2)}, u32[]{:S(2)}) async-start(bf16[4,96,2048]{2,1,0:T(8,128)(2,1)} %bitcast.63), calls=%async_computation.1 | async-start | bytes 3145728 | tf_op jit(solution)/shard_map/all_to_all | solution.py:180
  89.5 10.1 %all-to-all-done.1 = bf16[4,96,2048]{2,1,0:T(8,128)(2,1)S(1)} async-done(((bf16[4,96,2048]{2,1,0:T(8,128)(2,1)}), bf16[4,96,2048]{2,1,0:T(8,128)(2,1)S(1)}, u32[]{:S(2)}, u32[]{:S(2)}) %all-to-all-start.1) | async-done | bytes 1572896 | tf_op jit(solution)/shard_map/all_to_all | solution.py:180
  99.6 4.6 %all-to-all-start = ((bf16[128,8,256]{2,0,1:T(8,128)(2,1)}), bf16[128,8,256]{2,0,1:T(8,128)(2,1)S(1)}, u32[]{:S(2)}, u32[]{:S(2)}) async-start(bf16[128,8,256]{2,0,1:T(8,128)(2,1)} %copy.142), calls=%async_computation | async-start | bytes 1048576 | tf_op jit(solution)/shard_map/all_to_all | solution.py:131
  104.3 7.8 %fusion.4 = f32[768,1024]{1,0:T(8,128)} fusion(bf16[1,2048,1024]{2,1,0:T(8,128)(2,1)} %all-gather.11.cloned.1.call-done, bf16[384,2048]{1,0:T(8,128)(2,1)} %bitcast.67, bf16[384,2048]{1,0:T(8,128)(2,1)S(1)} %bitcast.360), kind=kOutput, calls=%fused_computation.4 | convolution fusion | flops 3227516928 | bytes 10485760 | tf_op jit(solution)/shard_map/dot_general | solution.py:31
  112.0 7.1 %all-gather.9.cloned.1.call-done = bf16[1,2048,1024]{2,1,0:T(8,128)(2,1)} async-done(((bf16[1,2048,256]{2,1,0:T(8,128)(2,1)}), bf16[1,2048,1024]{2,1,0:T(8,128)(2,1)}) %all-gather.9.cloned.1.call-update) | async-done | bytes 4194320 | tf_op jit(solution)/shard_map/all_gather | solution.py:203
  119.1 8.9 %multiply_convert_fusion = bf16[768,1024]{1,0:T(8,128)(2,1)} fusion(f32[768,1024]{1,0:T(8,128)} %fusion.4, bf16[1,2048,1024]{2,1,0:T(8,128)(2,1)} %all-gather.9.cloned.1.call-done, bf16[384,2048]{1,0:T(8,128)(2,1)} %bitcast.67, bf16[384,2048]{1,0:T(8,128)(2,1)S(1)} %bitcast.361), kind=kOutput, calls=%fused_computation.9 | convolution fusion | flops 3235381248 | bytes 12058624 | tf_op jit(solution)/shard_map/dot_general | solution.py:32
  128.0 37.6 %all-gather.13.cloned.1.call-done = bf16[1,2048,1024]{2,1,0:T(8,128)(2,1)} async-done(((bf16[1,2048,256]{2,1,0:T(8,128)(2,1)}), bf16[1,2048,1024]{2,1,0:T(8,128)(2,1)}) %all-gather.13.cloned.1.call-update) | async-done | bytes 4194320 | tf_op jit(solution)/shard_map/all_gather | solution.py:203
  165.5 5.4 %fusion.11 = bf16[384,2048]{1,0:T(8,128)(2,1)} fusion(bf16[1,2048,1024]{2,1,0:T(8,128)(2,1)} %all-gather.13.cloned.1.call-done, bf16[768,1024]{1,0:T(8,128)(2,1)} %multiply_convert_fusion), kind=kOutput, calls=%fused_computation.11 | convolution fusion | flops 1611399168 | bytes 6553600 | tf_op jit(solution)/shard_map/dot_general | solution.py:39
  170.9 3.6 %all-to-all-start.4 = ((bf16[4,96,2048]{2,1,0:T(8,128)(2,1)}), bf16[4,96,2048]{2,1,0:T(8,128)(2,1)S(1)}, u32[]{:S(2)}, u32[]{:S(2)}) async-start(bf16[4,96,2048]{2,1,0:T(8,128)(2,1)} %bitcast.75), calls=%async_computation.4 | async-start | bytes 3145728 | tf_op jit(solution)/shard_map/all_to_all | solution.py:180
  174.6 5.5 %fusion.8 = bf16[384,2048]{1,0:T(8,128)(2,1)} fusion(bf16[1,2048,1024]{2,1,0:T(8,128)(2,1)} %all-gather.13.cloned.1.call-done, bf16[768,1024]{1,0:T(8,128)(2,1)} %multiply_convert_fusion), kind=kOutput, calls=%fused_computation.10 | convolution fusion | flops 1611399168 | bytes 6553600 | tf_op jit(solution)/shard_map/dot_general | solution.py:39
  180.1 15.0 %all-to-all-done.4 = bf16[4,96,2048]{2,1,0:T(8,128)(2,1)S(1)} async-done(((bf16[4,96,2048]{2,1,0:T(8,128)(2,1)}), bf16[4,96,2048]{2,1,0:T(8,128)(2,1)S(1)}, u32[]{:S(2)}, u32[]{:S(2)}) %all-to-all-start.4) | async-done | bytes 1572896 | tf_op jit(solution)/shard_map/all_to_all | solution.py:180
  195.1 3.8 %all-to-all-start.3 = ((bf16[4,96,2048]{2,1,0:T(8,128)(2,1)}), bf16[4,96,2048]{2,1,0:T(8,128)(2,1)S(1)}, u32[]{:S(2)}, u32[]{:S(2)}) async-start(bf16[4,96,2048]{2,1,0:T(8,128)(2,1)} %bitcast.362), calls=%async_computation.3 | async-start | bytes 3145728 | tf_op jit(solution)/shard_map/all_to_all | solution.py:180
  199.7 4.6 %convolution_convert_fusion.2 = bf16[256,2048]{1,0:T(8,128)(2,1)} fusion(bf16[1024,256]{1,0:T(8,128)(2,1)} %bitcast.383, bf16[1024,2048]{1,0:T(8,128)(2,1)} %param.22), kind=kOutput, calls=%fused_computation.14 | convolution fusion | flops 1074266112 | bytes 5767168 | tf_op jit(solution)/shard_map/dot_general | solution.py:130
  206.1 2.4 %collective-permute-start.3 = (bf16[128,2048]{1,0:T(8,128)(2,1)}, bf16[128,2048]{1,0:T(8,128)(2,1)S(1)}, u32[]{:S(2)}, u32[]{:S(2)}) collective-permute-start(bf16[128,2048]{1,0:T(8,128)(2,1)} %add_convert_fusion.1), channel_id=1, source_target_pairs={{0,4},{1,5},{2,6},{3,7},{4,0},{5,1},{6,2},{7,3},{8,12},{9,13},{10,... | collective-permute-start | bytes 1572872 | tf_op jit(solution)/shard_map/ppermute | solution.py:233
  208.5 10.0 %all-to-all-done.3 = bf16[4,96,2048]{2,1,0:T(8,128)(2,1)S(1)} async-done(((bf16[4,96,2048]{2,1,0:T(8,128)(2,1)}), bf16[4,96,2048]{2,1,0:T(8,128)(2,1)S(1)}, u32[]{:S(2)}, u32[]{:S(2)}) %all-to-all-start.3) | async-done | bytes 1572896 | tf_op jit(solution)/shard_map/all_to_all | solution.py:180
  219.5 12.7 %collective-permute-done.3 = bf16[128,2048]{1,0:T(8,128)(2,1)S(1)} collective-permute-done((bf16[128,2048]{1,0:T(8,128)(2,1)}, bf16[128,2048]{1,0:T(8,128)(2,1)S(1)}, u32[]{:S(2)}, u32[]{:S(2)}) %collective-permute-start.3) | collective-permute-done | bytes 524320 | tf_op jit(solution)/shard_map/ppermute | solution.py:233
  (311 shorter events, 50.5 us)
Async XLA Ops:
  7.2 29.0 %copy-start = (bf16[16,64,64]{2,1,0:T(8,128)(2,1)S(1)}, bf16[16,64,64]{2,1,0:T(8,128)(2,1)}, u32[]{:S(2)}) copy-start(bf16[16,64,64]{2,1,0:T(8,128)(2,1)} %param.18) | copy-start | bytes 393220
  7.2 97.1 %all-gather.11.cloned.1.call-start = ((), (), s32[]{:S(2)}) async-start(), calls=%async_computation.6 | async-start | bytes 5242880 | tf_op jit(solution)/shard_map/all_gather | solution.py:203
  7.9 111.2 %all-gather.9.cloned.1.call-start = ((), (), s32[]{:S(2)}) async-start(), calls=%async_computation.5 | async-start | bytes 5242880 | tf_op jit(solution)/shard_map/all_gather | solution.py:203
  9.5 24.6 %collective-permute-start = (bf16[128,3]{1,0:T(8,128)(2,1)S(1)}, bf16[128,3]{1,0:T(8,128)(2,1)S(1)}, u32[]{:S(2)}, u32[]{:S(2)}) collective-permute-start(bf16[128,3]{1,0:T(8,128)(2,1)S(1)} %slice.415), channel_id=1, source_target_pairs={{0,8},{8,16},{16,24},{1,9},{9,17},{17,25},{2,10},{10,18},{18,26},{... | collective-permute-start | bytes 2312 | tf_op jit(solution)/shard_map/ppermute | solution.py:23
  17.9 55.8 %collective-permute-start.1 = (f32[128,4]{0,1:T(4,128)}, f32[128,4]{0,1:T(4,128)}, u32[]{:S(2)}, u32[]{:S(2)}) collective-permute-start(f32[128,4]{0,1:T(4,128)} %pad_maximum_fusion.15), channel_id=1, source_target_pairs={{0,4},{1,5},{2,6},{3,7},{4,0},{5,1},{6,2},{7,3},{8,12},{9,13},{10,... | collective-permute-start | bytes 6152 | tf_op jit(solution)/shard_map/ppermute | solution.py:208
  20.5 54.8 %collective-permute-start.2 = (bf16[128,2048]{1,0:T(8,128)(2,1)}, bf16[128,2048]{1,0:T(8,128)(2,1)}, u32[]{:S(2)}, u32[]{:S(2)}) collective-permute-start(bf16[128,2048]{1,0:T(8,128)(2,1)} %param.23), channel_id=1, source_target_pairs={{0,4},{1,5},{2,6},{3,7},{4,0},{5,1},{6,2},{7,3},{8,12},{9,13},{10,... | collective-permute-start | bytes 1572872 | tf_op jit(solution)/shard_map/ppermute | solution.py:209
  25.7 53.8 %all-to-all-start.2 = ((bf16[4,96,2048]{2,1,0:T(8,128)(2,1)}), bf16[4,96,2048]{2,1,0:T(8,128)(2,1)}, u32[]{:S(2)}, u32[]{:S(2)}) async-start(bf16[4,96,2048]{2,1,0:T(8,128)(2,1)} %bitcast.66), calls=%async_computation.2 | async-start | bytes 3145728 | tf_op jit(solution)/shard_map/all_to_all | solution.py:180
  30.2 135.3 %all-gather.13.cloned.1.call-start = ((), (), s32[]{:S(2)}) async-start(), calls=%async_computation.7 | async-start | bytes 5242880 | tf_op jit(solution)/shard_map/all_gather | solution.py:203
  51.6 11.6 %copy-start.18 = (f32[128,1,128]{0,1,2:T(1,128)S(1)}, f32[128,1,128]{0,1,2:T(1,128)}, u32[]{:S(2)}) copy-start(f32[128,1,128]{0,1,2:T(1,128)} %copy-done.17) | copy-start | bytes 196612
  51.6 11.6 %copy-start.32 = (f32[128,1,128]{0,1,2:T(1,128)S(1)}, f32[128,1,128]{0,1,2:T(1,128)}, u32[]{:S(2)}) copy-start(f32[128,1,128]{0,1,2:T(1,128)} %copy-done.31) | copy-start | bytes 196612
  51.8 11.5 %copy-start.16 = (f32[128,1,128]{0,1,2:T(1,128)S(1)}, f32[128,1,128]{0,1,2:T(1,128)}, u32[]{:S(2)}) copy-start(f32[128,1,128]{0,1,2:T(1,128)} %copy-done.15) | copy-start | bytes 196612
  52.3 11.0 %copy-start.30 = (f32[128,1,128]{0,1,2:T(1,128)S(1)}, f32[128,1,128]{0,1,2:T(1,128)}, u32[]{:S(2)}) copy-start(f32[128,1,128]{0,1,2:T(1,128)} %copy-done.29) | copy-start | bytes 196612
  58.1 13.9 %copy-start.26 = (f32[128,1,128]{0,1,2:T(1,128)S(1)}, f32[128,1,128]{0,1,2:T(1,128)}, u32[]{:S(2)}) copy-start(f32[128,1,128]{0,1,2:T(1,128)} %copy-done.25) | copy-start | bytes 196612
  59.4 12.7 %copy-start.10 = (f32[128,1,128]{0,1,2:T(1,128)S(1)}, f32[128,1,128]{0,1,2:T(1,128)}, u32[]{:S(2)}) copy-start(f32[128,1,128]{0,1,2:T(1,128)} %copy-done.9) | copy-start | bytes 196612
  59.4 12.7 %copy-start.24 = (f32[128,1,128]{0,1,2:T(1,128)S(1)}, f32[128,1,128]{0,1,2:T(1,128)}, u32[]{:S(2)}) copy-start(f32[128,1,128]{0,1,2:T(1,128)} %copy-done.23) | copy-start | bytes 196612
  59.5 12.7 %copy-start.20 = (f32[128,1,128]{0,1,2:T(1,128)S(1)}, f32[128,1,128]{0,1,2:T(1,128)}, u32[]{:S(2)}) copy-start(f32[128,1,128]{0,1,2:T(1,128)} %copy-done.19) | copy-start | bytes 196612
  72.2 12.1 %copy-start.34 = (f32[128,1,128]{0,1,2:T(1,128)S(1)}, f32[128,1,128]{0,1,2:T(1,128)}, u32[]{:S(2)}) copy-start(f32[128,1,128]{0,1,2:T(1,128)} %copy-done.33) | copy-start | bytes 196612
  79.5 20.1 %all-to-all-start.1 = ((bf16[4,96,2048]{2,1,0:T(8,128)(2,1)}), bf16[4,96,2048]{2,1,0:T(8,128)(2,1)S(1)}, u32[]{:S(2)}, u32[]{:S(2)}) async-start(bf16[4,96,2048]{2,1,0:T(8,128)(2,1)} %bitcast.63), calls=%async_computation.1 | async-start | bytes 3145728 | tf_op jit(solution)/shard_map/all_to_all | solution.py:180
  99.6 71.3 %all-to-all-start = ((bf16[128,8,256]{2,0,1:T(8,128)(2,1)}), bf16[128,8,256]{2,0,1:T(8,128)(2,1)S(1)}, u32[]{:S(2)}, u32[]{:S(2)}) async-start(bf16[128,8,256]{2,0,1:T(8,128)(2,1)} %copy.142), calls=%async_computation | async-start | bytes 1048576 | tf_op jit(solution)/shard_map/all_to_all | solution.py:131
  170.9 24.2 %all-to-all-start.4 = ((bf16[4,96,2048]{2,1,0:T(8,128)(2,1)}), bf16[4,96,2048]{2,1,0:T(8,128)(2,1)S(1)}, u32[]{:S(2)}, u32[]{:S(2)}) async-start(bf16[4,96,2048]{2,1,0:T(8,128)(2,1)} %bitcast.75), calls=%async_computation.4 | async-start | bytes 3145728 | tf_op jit(solution)/shard_map/all_to_all | solution.py:180
  195.1 23.3 %all-to-all-start.3 = ((bf16[4,96,2048]{2,1,0:T(8,128)(2,1)}), bf16[4,96,2048]{2,1,0:T(8,128)(2,1)S(1)}, u32[]{:S(2)}, u32[]{:S(2)}) async-start(bf16[4,96,2048]{2,1,0:T(8,128)(2,1)} %bitcast.362), calls=%async_computation.3 | async-start | bytes 3145728 | tf_op jit(solution)/shard_map/all_to_all | solution.py:180
  204.3 14.2 %copy-start.49 = (s32[128]{0:T(128)S(1)}, s32[128]{0:T(128)}, u32[]{:S(2)}) copy-start(s32[128]{0:T(128)} %copy-done.48) | copy-start | bytes 1540
  204.8 14.2 %copy-start.47 = (s32[128]{0:T(128)S(1)}, s32[128]{0:T(128)}, u32[]{:S(2)}) copy-start(s32[128]{0:T(128)} %copy-done.46) | copy-start | bytes 1540
  206.1 26.1 %collective-permute-start.3 = (bf16[128,2048]{1,0:T(8,128)(2,1)}, bf16[128,2048]{1,0:T(8,128)(2,1)S(1)}, u32[]{:S(2)}, u32[]{:S(2)}) collective-permute-start(bf16[128,2048]{1,0:T(8,128)(2,1)} %add_convert_fusion.1), channel_id=1, source_target_pairs={{0,4},{1,5},{2,6},{3,7},{4,0},{5,1},{6,2},{7,3},{8,12},{9,13},{10,... | collective-permute-start | bytes 1572872 | tf_op jit(solution)/shard_map/ppermute | solution.py:233
  (50 other events, 199.3 us)
Sparse Core Ops, SparseCore 0:
  9.5 57.1 all-gather.10
  68.3 50.7 all-gather.8
  120.6 44.8 all-gather.12

commit v2 on v1

--- a/solution.py
+++ b/solution.py
@@ -1,9 +1,12 @@
 import jax
 import jax.numpy as jnp
 from jax import lax
+from jax.experimental import pallas as pl
+from jax.experimental.pallas import tpu as pltpu
 from jax.sharding import PartitionSpec as P
 
 BLOCK = 64
+LANES = 128
 
 
 def entering_2(x, axis, combine, identity):
@@ -35,41 +38,76 @@
     return ((up_cut + 1.0) * gate_cut * jax.nn.sigmoid(1.702 * gate_cut)).astype(jnp.bfloat16)
 
 
-def down_product(units, down_piece):
-    return lax.dot_general(
-        units, down_piece, (((1,), (1,)), ((), ())), preferred_element_type=jnp.float32
-    )
-
-
-def segment_recurrence(decay, drive):
-    channels, positions = decay.shape
-    span = 16
-    seg_count = positions // span
-    decay_split = decay.reshape(channels, seg_count, span).transpose(0, 2, 1)
-    drive_split = drive.reshape(channels, seg_count, span).transpose(0, 2, 1)
-    run_state = jnp.zeros((channels, seg_count), jnp.float32)
-    run_decay = jnp.ones((channels, seg_count), jnp.float32)
-    state_list = []
-    decay_list = []
-    for offset in range(span):
-        run_state = decay_split[:, offset] * run_state + drive_split[:, offset]
-        run_decay = run_decay * decay_split[:, offset]
-        state_list.append(run_state)
-        decay_list.append(run_decay)
-    local_state = jnp.stack(state_list, axis=1)
-    local_decay = jnp.stack(decay_list, axis=1)
-    decay_upto, state_upto = lax.associative_scan(combine_pairs, (run_decay, run_state), axis=1)
-    decay_before = jnp.concatenate(
-        [jnp.ones((channels, 1), jnp.float32), decay_upto[:, :-1]], axis=1
-    )
-    state_before = jnp.concatenate(
-        [jnp.zeros((channels, 1), jnp.float32), state_upto[:, :-1]], axis=1
-    )
-    identity = (jnp.ones((channels,), jnp.float32), jnp.zeros((channels,), jnp.float32))
-    carried = entering_2((decay_upto[:, -1], state_upto[:, -1]), "ep", combine_pairs, identity)
-    entering = state_before + decay_before * carried[1][:, None]
-    state = local_state + local_decay * entering[:, None, :]
-    return state.transpose(0, 2, 1).reshape(channels, positions)
+def down_product(units, down_pieces):
+    total = None
+    for part, piece in zip(units, down_pieces):
+        term = lax.dot_general(
+            part, piece, (((1,), (1,)), ((), ())), preferred_element_type=jnp.float32
+        )
+        total = term if total is None else total + term
+    return total.astype(jnp.bfloat16)
+
+
+def minus_expm1(v):
+    series = 1.0 + v * (1.0 / 9.0)
+    for n in range(8, 1, -1):
+        series = 1.0 + v * (1.0 / n) * series
+    return jnp.where(v > -0.5, -v * series, 1.0 - jnp.exp(v))
+
+
+def mixer_kernel(
+    behind_ref, source_ref, taps_ref, maps_ref, speeds_ref, spike_ref, state_ref, decay_ref
+):
+    channels, positions = source_ref.shape
+    tap_count = taps_ref.shape[1]
+    lane = lax.broadcasted_iota(jnp.int32, (channels, LANES), 1)
+
+    def tile(index, carry):
+        before, decay_in, state_in = carry
+        here = pl.ds(pl.multiple_of(index * LANES, LANES), LANES)
+        values = source_ref[:, here].astype(jnp.float32)
+        running = None
+        for tap in range(tap_count):
+            back = tap_count - 1 - tap
+            moved = values
+            if back:
+                moved = jnp.where(
+                    lane >= back, pltpu.roll(values, back, 1), pltpu.roll(before, back, 1)
+                )
+            term = moved * taps_ref[:, tap : tap + 1]
+            running = term if running is None else running + term
+        conv_out = running.astype(jnp.bfloat16)
+        both = jnp.dot(maps_ref[...], conv_out, preferred_element_type=jnp.float32)
+        rate = 1.0 / (1.0 + jnp.exp(-both[:channels]))
+        inflow = 1.0 / (1.0 + jnp.exp(-both[channels:]))
+        exponent = -8.0 * rate * speeds_ref[...] + spike_ref[:, here]
+        state = jnp.sqrt(minus_expm1(2.0 * exponent)) * inflow * conv_out.astype(jnp.float32)
+        decay = jnp.exp(exponent)
+        step = 1
+        while step < LANES:
+            inside = lane >= step
+            state = decay * jnp.where(inside, pltpu.roll(state, step, 1), 0.0) + state
+            decay = decay * jnp.where(inside, pltpu.roll(decay, step, 1), 1.0)
+            step *= 2
+        state = state + decay * state_in
+        decay = decay * decay_in
+        state_ref[:, here] = state
+        decay_ref[:, here] = decay
+        return values, decay[:, LANES - 1 :], state[:, LANES - 1 :]
+
+    start = (
+        behind_ref[...].astype(jnp.float32),
+        jnp.ones((channels, 1), jnp.float32),
+        jnp.zeros((channels, 1), jnp.float32),
+    )
+    lax.fori_loop(0, positions // LANES, tile, start)
+
+
+def block_diagonal(maps):
+    count, rows, columns = maps.shape
+    same = jnp.eye(count, dtype=maps.dtype)
+    spread = maps.transpose(0, 2, 1)[:, :, None, :] * same[:, None, :, None]
+    return spread.reshape(count * columns, count * rows)
 
 
 def mixer_half(
@@ -85,43 +123,35 @@
     channels, positions = scan_source_values.shape
     tp_index = lax.axis_index("tp")
     first_chan = tp_index * channels
-    conv_local = lax.dynamic_slice_in_dim(
-        causal_filter_coefficients, first_chan, channels, 0
-    ).astype(jnp.float32)
-    tap_count = conv_local.shape[1]
-    rim_cells = from_behind(scan_source_values[:, positions - tap_count + 1 :], "ep", 1)
-    padded = jnp.concatenate([rim_cells, scan_source_values], axis=1).astype(jnp.float32)
-    running = padded[:, 0:positions] * conv_local[:, 0:1]
-    for shift_tap in range(1, tap_count):
-        running = (
-            running
-            + padded[:, shift_tap : shift_tap + positions]
-            * conv_local[:, shift_tap : shift_tap + 1]
-        )
-    conv_out = running.astype(jnp.bfloat16)
+    taps = lax.dynamic_slice_in_dim(causal_filter_coefficients, first_chan, channels, 0).astype(
+        jnp.float32
+    )
+    behind = from_behind(scan_source_values[:, positions - LANES :], "ep", 1)
     block_count = channels // BLOCK
-    rate_local = lax.dynamic_slice_in_dim(
-        scan_switch_blockmap, tp_index * block_count, block_count, 0
-    )
-    input_local = lax.dynamic_slice_in_dim(
-        entry_switch_blockmap, tp_index * block_count, block_count, 0
-    )
-    grouped = conv_out.reshape(block_count, BLOCK, positions)
-    block_dims = (((1,), (1,)), ((0,), (0,)))
-    scan_switch = jax.nn.sigmoid(
-        lax.dot_general(
-            rate_local, grouped, block_dims, preferred_element_type=jnp.float32
-        ).reshape(channels, positions)
-    )
-    inflow = jax.nn.sigmoid(
-        lax.dot_general(
-            input_local, grouped, block_dims, preferred_element_type=jnp.float32
-        ).reshape(channels, positions)
-    )
-    feature_fading = lax.dynamic_slice_in_dim(feature_fading_speeds, first_chan, channels, 0)
-    fading_exponent = -8.0 * scan_switch * feature_fading[:, None] + spike_amount[None, :]
-    drive = jnp.sqrt(-jnp.expm1(2.0 * fading_exponent)) * inflow * conv_out.astype(jnp.float32)
-    state = segment_recurrence(jnp.exp(fading_exponent), drive)
+    maps = jnp.concatenate(
+        [
+            block_diagonal(lax.dynamic_slice_in_dim(m, tp_index * block_count, block_count, 0))
+            for m in (scan_switch_blockmap, entry_switch_blockmap)
+        ],
+        axis=0,
+    )
+    speeds = lax.dynamic_slice_in_dim(feature_fading_speeds, first_chan, channels, 0)
+    whole = jax.ShapeDtypeStruct((channels, positions), jnp.float32)
+    local_state, local_decay = pl.pallas_call(
+        mixer_kernel,
+        out_shape=(whole, whole),
+        in_specs=[pl.BlockSpec(memory_space=pltpu.VMEM)] * 6,
+        out_specs=[pl.BlockSpec(memory_space=pltpu.VMEM)] * 2,
+        compiler_params=pltpu.CompilerParams(vmem_limit_bytes=16 * 1024 * 1024),
+        cost_estimate=pl.CostEstimate(
+            flops=400 * channels * positions,
+            bytes_accessed=10 * channels * positions,
+            transcendentals=0,
+        ),
+    )(behind, scan_source_values, taps, maps, speeds[:, None], spike_amount[None, :])
+    identity = (jnp.ones((channels,), jnp.float32), jnp.zeros((channels,), jnp.float32))
+    carried = entering_2((local_decay[:, -1], local_state[:, -1]), "ep", combine_pairs, identity)
+    state = local_state + local_decay * carried[1][:, None]
     mix_hidden = (
         state * jax.nn.gelu(switch_path_values.astype(jnp.float32), approximate=True)
     ).astype(jnp.bfloat16)
@@ -197,19 +227,25 @@
     tp_count = lax.axis_size("tp")
     half = tp_count // 2
     swap = [(i, (i + half) % tp_count) for i in range(tp_count)]
-    halves = [list(range(half)), list(range(half, tp_count))]
-
-    def gather_half(piece):
-        return lax.all_gather(piece, "tp", axis=1, tiled=True, axis_index_groups=halves)
+
+    def half_pieces(piece):
+        bit = half // 2
+        while bit:
+            other = lax.ppermute(piece, "tp", [(i, i ^ bit) for i in range(tp_count)])
+            if bit == 1:
+                return [piece, other]
+            piece = jnp.concatenate([piece, other], axis=1)
+            bit //= 2
+        return [piece]
 
     table = jnp.concatenate(
         [selected_specialist_ids.astype(jnp.float32), selected_specialist_share], axis=1
     )
     far_table = lax.ppermute(table, "tp", swap)
     far_activity = lax.ppermute(dispatched_group_activity, "tp", swap)
-    gate_full = gather_half(specialist_switch_maps[0])
-    up_full = gather_half(specialist_widen_maps[0])
-    down_full = gather_half(specialist_shrink_maps[0])
+    gate_pieces = half_pieces(specialist_switch_maps[0])
+    up_pieces = half_pieces(specialist_widen_maps[0])
+    down_pieces = half_pieces(specialist_shrink_maps[0])
 
     near_places = slot_places(selected_specialist_ids, expert_count, slot_count)
     near_rows = rows_in_slots(
@@ -224,10 +260,10 @@
     )
     far_arrived = over_experts(far_rows, expert_count)
     arrived = jnp.concatenate([far_arrived, near_arrived], axis=0)
-    units = expert_units(arrived, gate_full, up_full)
-    far_result = down_product(units[:slot_total], down_full).astype(jnp.bfloat16)
+    units = [expert_units(arrived, g, u) for g, u in zip(gate_pieces, up_pieces)]
+    far_result = down_product([part[:slot_total] for part in units], down_pieces)
     far_returned = over_experts(far_result, expert_count)
-    near_result = down_product(units[slot_total:], down_full).astype(jnp.bfloat16)
+    near_result = down_product([part[slot_total:] for part in units], down_pieces)
     near_returned = over_experts(near_result, expert_count)
     far_sum = weighted_routes(far_returned, far_places, far_share).astype(jnp.bfloat16)
     home_sum = lax.ppermute(far_sum, "tp", swap)

time: 241 us -> 191 us (0.79)
  waiting for transfers between devices: 94.5 us -> 64 us
  Pallas kernels: 0 us -> 16.7 us
  local copies, waits for them, and re-layouts: 21 us -> 4.58 us
  between operations: 15.3 us -> 0.97 us
  other arithmetic: 25.7 us -> 15.7 us
  starting transfers between devices: 30.6 us -> 36.6 us
    all_gather x3 -> x0, waiting for transfers between devices: 44.7 us -> none  [gather_half(): lax.all_gather(piece, 'tp', axis=1, tiled=True, axis_index_groups=halves)]
    ppermute x0 -> x6, waiting for transfers between devices: none -> 21.3 us  [half_pieces(): other = lax.ppermute(piece, 'tp', [(i, i ^ bit) for i in range(tp_count)])]
    pallas_call x0 -> x1, Pallas kernels: none -> 16.7 us  [mixer_half(): pl.pallas_call(mixer_kernel, out_shape=(whole, whole), in_specs=[pl.Block...]
    all_to_all x4, waiting for transfers between devices: 35.1 us -> 23.5 us  [over_experts(): lax.all_to_all(pieces, 'ep', split_axis=0, concat_axis=0, tiled=True)]
    concatenate x12 -> x4, other arithmetic: 0.1 us -> 9.1 us  [the longest x3 9.09 us: half_pieces(): piece = jnp.concatenate([piece, other], axis=1)]
    ppermute x1, waiting for transfers between devices: 0.01 us -> 7.26 us  [from_behind(): return lax.ppermute(x, axis, pairs)]
    add x27 -> x0, other arithmetic: 5.38 us -> none  [the longest x13 3.02 us: segment_recurrence(): lax.associative_scan(combine_pairs, (run_decay, run_state), axis=1)]
    div x2 -> x0, local copies, waits for them, and re-layouts: 4.79 us -> none  [mixer_half(): jax.nn.sigmoid(lax.dot_general(rate_local, grouped, block_dims, preferred...]
  transfers between devices with their start and end apart: 12 -> 15, of which waited for: 6 -> 6; matrix products, arithmetic and copies ran while one was open for 37% -> 30% of each run, Pallas kernels for 0% -> 9%
where the time goes in v2:
time: 191 us; the launch traced here: 190 us
  waiting for transfers between devices  64 us (34%)
  matrix products  41.6 us (22%)
  starting transfers between devices  36.6 us (19%)
  Pallas kernels  16.7 us (9%)
  other arithmetic  15.7 us (8%)
  blocking collectives  10.2 us (5%)
  local copies, waits for them, and re-layouts  4.58 us (2%)
    all_to_all x4, waiting for transfers between devices, over_experts(): lax.all_to_all(pieces, 'ep', split_axis=0, concat_axis=0, tiled=True)  23.5 us
    ppermute x6, waiting for transfers between devices, half_pieces(): other = lax.ppermute(piece, 'tp', [(i, i ^ bit) for i in range(tp_count)])  21.3 us
    pallas_call x1, Pallas kernels, mixer_half(): pl.pallas_call(mixer_kernel, out_shape=(whole, whole), in_specs=[pl.Block...  16.7 us
    all_to_all x4, starting transfers between devices, over_experts(): lax.all_to_all(pieces, 'ep', split_axis=0, concat_axis=0, tiled=True)  16.2 us
    ppermute x1, waiting for transfers between devices, expert_half(): home_sum = lax.ppermute(far_sum, 'tp', swap)  11.9 us
    dot_general x4, matrix products, down_product(): lax.dot_general(part, piece, (((1,), (1,)), ((), ())), preferred_element_...  11.2 us
    all_gather x1, blocking collectives, entering_2(): packed = lax.all_gather(jnp.stack(x), axis)  10.2 us
    dot_general x2, matrix products, expert_units(): gate_pre = jnp.dot(rows, gate_piece, preferred_element_type=jnp.float32)  9.37 us
  transfers between devices with their start and end apart: 15, of which 6 were waited for; matrix products, arithmetic and copies ran while one was open for 30% of the time, Pallas kernels for 9%

profile of v2, /device:TPU:0, one launch (start us, length us, event | category | flops | bytes accessed | tf_op | source)
XLA Modules:
  0.0 190.4 jit_solution(12961198503459493279)
XLA Ops:
  3.6 4.1 %collective-permute-start.1 = (f32[128,4]{0,1:T(4,128)S(1)}, f32[128,4]{0,1:T(4,128)S(1)}, u32[]{:S(2)}, u32[]{:S(2)}) collective-permute-start(f32[128,4]{0,1:T(4,128)S(1)} %pad_maximum_fusion.5), channel_id=1, source_target_pairs={{0,4},{1,5},{2,6},{3,7},{4,0},{5,1},{6,2},{7,3},{8,12},{9,13},{10,... | collective-permute-start | bytes 6152 | tf_op jit(solution)/shard_map/ppermute | solution.py:244
  12.7 4.5 %all-to-all-start.2 = ((bf16[4,96,2048]{2,1,0:T(8,128)(2,1)}), bf16[4,96,2048]{2,1,0:T(8,128)(2,1)}, u32[]{:S(2)}, u32[]{:S(2)}) async-start(bf16[4,96,2048]{2,1,0:T(8,128)(2,1)} %bitcast.21), calls=%async_computation.2 | async-start | bytes 3145728 | tf_op jit(solution)/shard_map/all_to_all | solution.py:210
  23.6 3.8 %collective-permute-start = (bf16[128,128]{1,0:T(8,128)(2,1)S(1)}, bf16[128,128]{1,0:T(8,128)(2,1)S(1)}, u32[]{:S(2)}, u32[]{:S(2)}) collective-permute-start(bf16[128,128]{1,0:T(8,128)(2,1)S(1)} %slice.79), channel_id=1, source_target_pairs={{0,8},{8,16},{16,24},{1,9},{9,17},{17,25},{2,10},{10,18},{18,26},{... | collective-permute-start | bytes 98312 | tf_op jit(solution)/shard_map/ppermute | solution.py:26
  27.6 7.3 %collective-permute-done.behind_ref = bf16[128,128]{1,0:T(8,128)(2,1)S(1)} collective-permute-done((bf16[128,128]{1,0:T(8,128)(2,1)S(1)}, bf16[128,128]{1,0:T(8,128)(2,1)S(1)}, u32[]{:S(2)}, u32[]{:S(2)}) %collective-permute-start) | collective-permute-done | bytes 32800 | tf_op jit(solution)/shard_map/ppermute | solution.py:26
  34.9 16.7 %shard_map.158 = (f32[128,2048]{1,0:T(8,128)S(1)}, f32[128,2048]{1,0:T(8,128)S(1)}) custom-call(bf16[128,128]{1,0:T(8,128)(2,1)S(1)} %collective-permute-done.behind_ref, bf16[128,2048]{1,0:T(8,128)(2,1)S(1)} %copy-done.1, f32[128,4]{1,0:T(8,128)S(1)} %convert_element_type.101.taps_ref, bf16[256,128]{1,0:T(8,128)(2,1)S(1)} %pad_maximum_fusion.4.maps_ref, ...), custom_call_target="tpu_custom_call" | custom-call | flops 104857600 | bytes 2621440 | tf_op jit(solution)/shard_map/pallas_call | solution.py:140
  52.0 10.2 %all-gather.1 = f32[4,2,128]{2,1,0:T(2,128)S(1)} all-gather(f32[1,2,128]{2,1,0:T(2,128)S(1)} %maximum_bitcast_fusion), channel_id=2, replica_groups=mesh['ep'=4,'tp'=8] {'ep'}, dimensions={0}, use_global_device_ids=true | all-gather | bytes 5120 | tf_op jit(solution)/shard_map/all_gather | solution.py:14
  64.2 4.3 %all-to-all-start.1 = ((bf16[4,96,2048]{2,1,0:T(8,128)(2,1)}), bf16[4,96,2048]{2,1,0:T(8,128)(2,1)}, u32[]{:S(2)}, u32[]{:S(2)}) async-start(bf16[4,96,2048]{2,1,0:T(8,128)(2,1)} %bitcast.114), calls=%async_computation.1 | async-start | bytes 3145728 | tf_op jit(solution)/shard_map/all_to_all | solution.py:210
  71.6 4.6 %collective-permute-done.4 = bf16[2048,256]{1,0:T(8,128)(2,1)} collective-permute-done((bf16[2048,256]{1,0:T(8,128)(2,1)}, bf16[2048,256]{1,0:T(8,128)(2,1)}, u32[]{:S(2)}, u32[]{:S(2)}) %collective-permute-start.4) | collective-permute-done | bytes 1048608 | tf_op jit(solution)/shard_map/ppermute | solution.py:234
  76.2 3.1 %pad_maximum_fusion.2 = bf16[2048,512]{1,0:T(8,128)(2,1)} fusion(bf16[2048,256]{1,0:T(8,128)(2,1)} %collective-permute-done.4, bf16[2048,256]{1,0:T(8,128)(2,1)} %bitcast.24), kind=kLoop, calls=%fused_computation.10 | loop fusion | flops 4194304 | bytes 4194304 | tf_op jit(solution)/shard_map/concatenate | solution.py:237
  80.6 16.7 %collective-permute-done.5 = bf16[2048,256]{1,0:T(8,128)(2,1)} collective-permute-done((bf16[2048,256]{1,0:T(8,128)(2,1)}, bf16[2048,256]{1,0:T(8,128)(2,1)}, u32[]{:S(2)}, u32[]{:S(2)}) %collective-permute-start.5) | collective-permute-done | bytes 1048608 | tf_op jit(solution)/shard_map/ppermute | solution.py:234
  97.2 3.0 %pad_maximum_fusion.3 = bf16[2048,512]{1,0:T(8,128)(2,1)} fusion(bf16[2048,256]{1,0:T(8,128)(2,1)} %collective-permute-done.5, bf16[2048,256]{1,0:T(8,128)(2,1)} %bitcast.25), kind=kLoop, calls=%fused_computation.11 | loop fusion | flops 4194304 | bytes 4194304 | tf_op jit(solution)/shard_map/concatenate | solution.py:237
  100.3 6.0 %all-to-all-start = ((bf16[128,8,256]{2,0,1:T(8,128)(2,1)}), bf16[128,8,256]{2,0,1:T(8,128)(2,1)S(1)}, u32[]{:S(2)}, u32[]{:S(2)}) async-start(bf16[128,8,256]{2,0,1:T(8,128)(2,1)} %bitcast.108), calls=%async_computation | async-start | bytes 1048576 | tf_op jit(solution)/shard_map/all_to_all | solution.py:161
  106.2 4.3 %fusion.54 = f32[768,512]{1,0:T(8,128)S(1)} fusion(bf16[384,2048]{1,0:T(8,128)(2,1)} %bitcast.22, bf16[384,2048]{1,0:T(8,128)(2,1)} %bitcast.19, bf16[2048,256]{1,0:T(8,128)(2,1)} %collective-permute-done.3, bf16[2048,256]{1,0:T(8,128)(2,1)} %bitcast.23), kind=kOutput, calls=%fused_computation.124 | convolution fusion | flops 1621098496 | bytes 6815744 | tf_op jit(solution)/shard_map/dot_general | solution.py:35
  110.5 4.7 %multiply_convert_fusion.1 = bf16[768,512]{1,0:T(8,128)(2,1)S(1)} fusion(f32[768,512]{1,0:T(8,128)S(1)} %fusion.54, bf16[384,2048]{1,0:T(8,128)(2,1)} %bitcast.22, bf16[384,2048]{1,0:T(8,128)(2,1)} %bitcast.19, bf16[2048,256]{1,0:T(8,128)(2,1)} %collective-permute-done.4, bf16[2048,256]{1,0:T(8,128)(2,1)} %bitcast.24), kind=kOutput, calls=%fused_computation.17 | convolution fusion | flops 1625030656 | bytes 7602176 | tf_op jit(solution)/shard_map/dot_general | solution.py:34
  115.2 4.3 %fusion.53 = f32[768,512]{1,0:T(8,128)S(1)} fusion(bf16[2048,512]{1,0:T(8,128)(2,1)} %collective-permute-done.6, bf16[384,2048]{1,0:T(8,128)(2,1)} %bitcast.22, bf16[384,2048]{1,0:T(8,128)(2,1)} %bitcast.19), kind=kOutput, calls=%fused_computation.123 | convolution fusion | flops 1616904192 | bytes 6815744 | tf_op jit(solution)/shard_map/dot_general | solution.py:35
  119.5 4.7 %multiply_convert_fusion = bf16[768,512]{1,0:T(8,128)(2,1)S(1)} fusion(f32[768,512]{1,0:T(8,128)S(1)} %fusion.53, bf16[2048,512]{1,0:T(8,128)(2,1)} %collective-permute-done.7, bf16[384,2048]{1,0:T(8,128)(2,1)} %bitcast.22, bf16[384,2048]{1,0:T(8,128)(2,1)} %bitcast.19), kind=kOutput, calls=%fused_computation.16 | convolution fusion | flops 1620836352 | bytes 7602176 | tf_op jit(solution)/shard_map/dot_general | solution.py:34
  126.5 3.7 %add_convert_fusion = bf16[384,2048]{1,0:T(8,128)(2,1)} fusion(f32[384,2048]{1,0:T(8,128)S(1)} %fusion.20, bf16[768,512]{1,0:T(8,128)(2,1)S(1)} %multiply_convert_fusion.1, bf16[2048,256]{1,0:T(8,128)(2,1)} %collective-permute-done.5, bf16[2048,256]{1,0:T(8,128)(2,1)} %bitcast.25), kind=kOutput, calls=%fused_computation.1 | convolution fusion | flops 811073536 | bytes 7208960 | tf_op jit(solution)/shard_map/dot_general | solution.py:44
  130.2 3.8 %all-to-all-start.4 = ((bf16[4,96,2048]{2,1,0:T(8,128)(2,1)}), bf16[4,96,2048]{2,1,0:T(8,128)(2,1)S(1)}, u32[]{:S(2)}, u32[]{:S(2)}) async-start(bf16[4,96,2048]{2,1,0:T(8,128)(2,1)} %bitcast.116), calls=%async_computation.4 | async-start | bytes 3145728 | tf_op jit(solution)/shard_map/all_to_all | solution.py:210
  136.8 3.7 %add_convert_fusion.1 = bf16[384,2048]{1,0:T(8,128)(2,1)} fusion(f32[384,2048]{1,0:T(8,128)S(1)} %fusion.23, bf16[768,512]{1,0:T(8,128)(2,1)S(1)} %multiply_convert_fusion.1, bf16[2048,256]{1,0:T(8,128)(2,1)} %collective-permute-done.5, bf16[2048,256]{1,0:T(8,128)(2,1)} %bitcast.25), kind=kOutput, calls=%fused_computation.2 | convolution fusion | flops 811073536 | bytes 7208960 | tf_op jit(solution)/shard_map/dot_general | solution.py:44
  140.5 13.4 %all-to-all-done.4 = bf16[4,96,2048]{2,1,0:T(8,128)(2,1)S(1)} async-done(((bf16[4,96,2048]{2,1,0:T(8,128)(2,1)}), bf16[4,96,2048]{2,1,0:T(8,128)(2,1)S(1)}, u32[]{:S(2)}, u32[]{:S(2)}) %all-to-all-start.4) | async-done | bytes 1572896 | tf_op jit(solution)/shard_map/all_to_all | solution.py:210
  153.9 3.6 %all-to-all-start.3 = ((bf16[4,96,2048]{2,1,0:T(8,128)(2,1)}), bf16[4,96,2048]{2,1,0:T(8,128)(2,1)S(1)}, u32[]{:S(2)}, u32[]{:S(2)}) async-start(bf16[4,96,2048]{2,1,0:T(8,128)(2,1)} %bitcast.115), calls=%async_computation.3 | async-start | bytes 3145728 | tf_op jit(solution)/shard_map/all_to_all | solution.py:210
  157.5 4.6 %convolution_convert_fusion.2 = bf16[256,2048]{1,0:T(8,128)(2,1)} fusion(bf16[1024,256]{1,0:T(8,128)(2,1)} %bitcast.118, bf16[1024,2048]{1,0:T(8,128)(2,1)} %param.22), kind=kOutput, calls=%fused_computation.5 | convolution fusion | flops 1074266112 | bytes 5767168 | tf_op jit(solution)/shard_map/dot_general | solution.py:160
  166.4 10.1 %all-to-all-done.3 = bf16[4,96,2048]{2,1,0:T(8,128)(2,1)S(1)} async-done(((bf16[4,96,2048]{2,1,0:T(8,128)(2,1)}), bf16[4,96,2048]{2,1,0:T(8,128)(2,1)S(1)}, u32[]{:S(2)}, u32[]{:S(2)}) %all-to-all-start.3) | async-done | bytes 1572896 | tf_op jit(solution)/shard_map/all_to_all | solution.py:210
  177.5 11.9 %collective-permute-done.9 = bf16[128,2048]{1,0:T(8,128)(2,1)S(1)} collective-permute-done((bf16[128,2048]{1,0:T(8,128)(2,1)}, bf16[128,2048]{1,0:T(8,128)(2,1)S(1)}, u32[]{:S(2)}, u32[]{:S(2)}) %collective-permute-start.9) | collective-permute-done | bytes 524320 | tf_op jit(solution)/shard_map/ppermute | solution.py:269
  (82 shorter events, 32.4 us)
Async XLA Ops:
  0.6 21.9 %copy-start = (bf16[1024,4]{0,1:T(4,128)(2,1)S(1)}, bf16[1024,4]{0,1:T(4,128)(2,1)}, u32[]{:S(2)}) copy-start(bf16[1024,4]{0,1:T(4,128)(2,1)} %param.17) | copy-start | bytes 24580
  3.6 19.9 %collective-permute-start.1 = (f32[128,4]{0,1:T(4,128)S(1)}, f32[128,4]{0,1:T(4,128)S(1)}, u32[]{:S(2)}, u32[]{:S(2)}) collective-permute-start(f32[128,4]{0,1:T(4,128)S(1)} %pad_maximum_fusion.5), channel_id=1, source_target_pairs={{0,4},{1,5},{2,6},{3,7},{4,0},{5,1},{6,2},{7,3},{8,12},{9,13},{10,... | collective-permute-start | bytes 6152 | tf_op jit(solution)/shard_map/ppermute | solution.py:244
  7.7 54.5 %collective-permute-start.2 = (bf16[128,2048]{1,0:T(8,128)(2,1)}, bf16[128,2048]{1,0:T(8,128)(2,1)S(1)}, u32[]{:S(2)}, u32[]{:S(2)}) collective-permute-start(bf16[128,2048]{1,0:T(8,128)(2,1)} %param.23), channel_id=1, source_target_pairs={{0,4},{1,5},{2,6},{3,7},{4,0},{5,1},{6,2},{7,3},{8,12},{9,13},{10,... | collective-permute-start | bytes 1572872 | tf_op jit(solution)/shard_map/ppermute | solution.py:245
  12.7 10.9 %copy-start.1 = (bf16[128,2048]{1,0:T(8,128)(2,1)S(1)}, bf16[128,2048]{1,0:T(8,128)(2,1)}, u32[]{:S(2)}) copy-start(bf16[128,2048]{1,0:T(8,128)(2,1)} %source_ref.1) | copy-start | bytes 1572868
  12.7 22.2 %copy-start.2 = (f32[2048]{0:T(1024)S(1)}, f32[2048]{0:T(1024)}, u32[]{:S(2)}) copy-start(f32[2048]{0:T(1024)} %param.21) | copy-start | bytes 24580
  12.7 51.5 %all-to-all-start.2 = ((bf16[4,96,2048]{2,1,0:T(8,128)(2,1)}), bf16[4,96,2048]{2,1,0:T(8,128)(2,1)}, u32[]{:S(2)}, u32[]{:S(2)}) async-start(bf16[4,96,2048]{2,1,0:T(8,128)(2,1)} %bitcast.21), calls=%async_computation.2 | async-start | bytes 3145728 | tf_op jit(solution)/shard_map/all_to_all | solution.py:210
  17.2 51.4 %collective-permute-start.3 = (bf16[2048,256]{1,0:T(8,128)(2,1)}, bf16[2048,256]{1,0:T(8,128)(2,1)}, u32[]{:S(2)}, u32[]{:S(2)}) collective-permute-start(bf16[2048,256]{1,0:T(8,128)(2,1)} %bitcast.23), channel_id=1, source_target_pairs={{0,2},{1,3},{2,0},{3,1},{4,6},{5,7},{6,4},{7,5},{8,10},{9,11},{10,... | collective-permute-start | bytes 3145736 | tf_op jit(solution)/shard_map/ppermute | solution.py:234
  19.1 57.1 %collective-permute-start.4 = (bf16[2048,256]{1,0:T(8,128)(2,1)}, bf16[2048,256]{1,0:T(8,128)(2,1)}, u32[]{:S(2)}, u32[]{:S(2)}) collective-permute-start(bf16[2048,256]{1,0:T(8,128)(2,1)} %bitcast.24), channel_id=1, source_target_pairs={{0,2},{1,3},{2,0},{3,1},{4,6},{5,7},{6,4},{7,5},{8,10},{9,11},{10,... | collective-permute-start | bytes 3145736 | tf_op jit(solution)/shard_map/ppermute | solution.py:234
  19.3 78.0 %collective-permute-start.5 = (bf16[2048,256]{1,0:T(8,128)(2,1)}, bf16[2048,256]{1,0:T(8,128)(2,1)}, u32[]{:S(2)}, u32[]{:S(2)}) collective-permute-start(bf16[2048,256]{1,0:T(8,128)(2,1)} %bitcast.25), channel_id=1, source_target_pairs={{0,2},{1,3},{2,0},{3,1},{4,6},{5,7},{6,4},{7,5},{8,10},{9,11},{10,... | collective-permute-start | bytes 3145736 | tf_op jit(solution)/shard_map/ppermute | solution.py:234
  23.6 11.3 %collective-permute-start = (bf16[128,128]{1,0:T(8,128)(2,1)S(1)}, bf16[128,128]{1,0:T(8,128)(2,1)S(1)}, u32[]{:S(2)}, u32[]{:S(2)}) collective-permute-start(bf16[128,128]{1,0:T(8,128)(2,1)S(1)} %slice.79), channel_id=1, source_target_pairs={{0,8},{8,16},{16,24},{1,9},{9,17},{17,25},{2,10},{10,18},{18,26},{... | collective-permute-start | bytes 98312 | tf_op jit(solution)/shard_map/ppermute | solution.py:26
  64.2 36.0 %all-to-all-start.1 = ((bf16[4,96,2048]{2,1,0:T(8,128)(2,1)}), bf16[4,96,2048]{2,1,0:T(8,128)(2,1)}, u32[]{:S(2)}, u32[]{:S(2)}) async-start(bf16[4,96,2048]{2,1,0:T(8,128)(2,1)} %bitcast.114), calls=%async_computation.1 | async-start | bytes 3145728 | tf_op jit(solution)/shard_map/all_to_all | solution.py:210
  71.6 7.6 %copy-start.6 = (bf16[128,2048]{1,0:T(8,128)(2,1)S(1)}, bf16[128,2048]{1,0:T(8,128)(2,1)}, u32[]{:S(2)}) copy-start(bf16[128,2048]{1,0:T(8,128)(2,1)} %param.16) | copy-start | bytes 1572868
  71.6 43.6 %collective-permute-start.6 = (bf16[2048,512]{1,0:T(8,128)(2,1)}, bf16[2048,512]{1,0:T(8,128)(2,1)}, u32[]{:S(2)}, u32[]{:S(2)}) collective-permute-start(bf16[2048,512]{1,0:T(8,128)(2,1)} %pad_maximum_fusion.1), channel_id=1, source_target_pairs={{0,1},{1,0},{2,3},{3,2},{4,5},{5,4},{6,7},{7,6},{8,9},{9,8},{10,11... | collective-permute-start | bytes 6291464 | tf_op jit(solution)/shard_map/ppermute | solution.py:234
  79.2 40.3 %collective-permute-start.7 = (bf16[2048,512]{1,0:T(8,128)(2,1)}, bf16[2048,512]{1,0:T(8,128)(2,1)}, u32[]{:S(2)}, u32[]{:S(2)}) collective-permute-start(bf16[2048,512]{1,0:T(8,128)(2,1)} %pad_maximum_fusion.2), channel_id=1, source_target_pairs={{0,1},{1,0},{2,3},{3,2},{4,5},{5,4},{6,7},{7,6},{8,9},{9,8},{10,11... | collective-permute-start | bytes 6291464 | tf_op jit(solution)/shard_map/ppermute | solution.py:234
  100.3 24.0 %collective-permute-start.8 = (bf16[2048,512]{1,0:T(8,128)(2,1)}, bf16[2048,512]{1,0:T(8,128)(2,1)S(1)}, u32[]{:S(2)}, u32[]{:S(2)}) collective-permute-start(bf16[2048,512]{1,0:T(8,128)(2,1)} %pad_maximum_fusion.3), channel_id=1, source_target_pairs={{0,1},{1,0},{2,3},{3,2},{4,5},{5,4},{6,7},{7,6},{8,9},{9,8},{10,11... | collective-permute-start | bytes 6291464 | tf_op jit(solution)/shard_map/ppermute | solution.py:234
  100.3 29.9 %all-to-all-start = ((bf16[128,8,256]{2,0,1:T(8,128)(2,1)}), bf16[128,8,256]{2,0,1:T(8,128)(2,1)S(1)}, u32[]{:S(2)}, u32[]{:S(2)}) async-start(bf16[128,8,256]{2,0,1:T(8,128)(2,1)} %bitcast.108), calls=%async_computation | async-start | bytes 1048576 | tf_op jit(solution)/shard_map/all_to_all | solution.py:161
  124.2 0.9 copy-start.4
  125.1 1.3 copy-start.3
  130.2 3.8 %copy-start.7 = (f32[128,2]{0,1:T(2,128)S(1)}, f32[128,2]{0,1:T(2,128)}, u32[]{:S(2)}) copy-start(f32[128,2]{0,1:T(2,128)} %param.26) | copy-start | bytes 3076
  130.2 6.6 %copy-start.5 = (bf16[128,8,256]{2,0,1:T(8,128)(2,1)}, bf16[128,8,256]{2,0,1:T(8,128)(2,1)S(1)}, u32[]{:S(2)}) copy-start(bf16[128,8,256]{2,0,1:T(8,128)(2,1)S(1)} %all-to-all-done) | copy-start | bytes 1572868
  130.2 23.7 %all-to-all-start.4 = ((bf16[4,96,2048]{2,1,0:T(8,128)(2,1)}), bf16[4,96,2048]{2,1,0:T(8,128)(2,1)S(1)}, u32[]{:S(2)}, u32[]{:S(2)}) async-start(bf16[4,96,2048]{2,1,0:T(8,128)(2,1)} %bitcast.116), calls=%async_computation.4 | async-start | bytes 3145728 | tf_op jit(solution)/shard_map/all_to_all | solution.py:210
  153.9 22.6 %all-to-all-start.3 = ((bf16[4,96,2048]{2,1,0:T(8,128)(2,1)}), bf16[4,96,2048]{2,1,0:T(8,128)(2,1)S(1)}, u32[]{:S(2)}, u32[]{:S(2)}) async-start(bf16[4,96,2048]{2,1,0:T(8,128)(2,1)} %bitcast.115), calls=%async_computation.3 | async-start | bytes 3145728 | tf_op jit(solution)/shard_map/all_to_all | solution.py:210
  163.9 25.6 %collective-permute-start.9 = (bf16[128,2048]{1,0:T(8,128)(2,1)}, bf16[128,2048]{1,0:T(8,128)(2,1)S(1)}, u32[]{:S(2)}, u32[]{:S(2)}) collective-permute-start(bf16[128,2048]{1,0:T(8,128)(2,1)} %add_convert_fusion.3), channel_id=1, source_target_pairs={{0,4},{1,5},{2,6},{3,7},{4,0},{5,1},{6,2},{7,3},{8,12},{9,13},{10,... | collective-permute-start | bytes 1572872 | tf_op jit(solution)/shard_map/ppermute | solution.py:269

commit v3 on v2

--- a/solution.py
+++ b/solution.py
@@ -219,7 +219,7 @@
     specialist_widen_maps,
     specialist_shrink_maps,
 ):
-    token_count, model_width = dispatched_group_activity.shape
+    token_count, _ = dispatched_group_activity.shape
     route_count = selected_specialist_ids.shape[1]
     expert_count = lax.axis_size("ep")
     slot_count = 3 * route_count * token_count // (2 * expert_count)
@@ -248,9 +248,8 @@
     down_pieces = half_pieces(specialist_shrink_maps[0])
 
     near_places = slot_places(selected_specialist_ids, expert_count, slot_count)
-    near_rows = rows_in_slots(
-        normed_rows(dispatched_group_activity, specialist_rmsgain), near_places, slot_total
-    )
+    near_normed = normed_rows(dispatched_group_activity, specialist_rmsgain)
+    near_rows = rows_in_slots(near_normed, near_places, slot_total)
     near_arrived = over_experts(near_rows, expert_count)
     far_ids = far_table[:, :route_count].astype(jnp.int32)
     far_share = far_table[:, route_count:]
@@ -329,6 +328,7 @@
         P("ep", None, "tp"),
     )
     out_specs = (P(("ep", "tp"), None), P(("ep", "tp"), None))
+
     return jax.shard_map(
         on_device, mesh=mesh, in_specs=in_specs, out_specs=out_specs, check_vma=False
     )

time: 191 us -> 191 us (level)
  no operation moved by 1% of the time
where the time goes in v3:
time: 191 us; the launch traced here: 190 us
  waiting for transfers between devices  64 us (34%)
  matrix products  41.6 us (22%)
  starting transfers between devices  36.6 us (19%)
  Pallas kernels  16.7 us (9%)
  other arithmetic  15.7 us (8%)
  blocking collectives  10.2 us (5%)
  local copies, waits for them, and re-layouts  4.58 us (2%)
    all_to_all x4, waiting for transfers between devices, over_experts(): lax.all_to_all(pieces, 'ep', split_axis=0, concat_axis=0, tiled=True)  23.5 us
    ppermute x6, waiting for transfers between devices, half_pieces(): other = lax.ppermute(piece, 'tp', [(i, i ^ bit) for i in range(tp_count)])  21.3 us
    pallas_call x1, Pallas kernels, mixer_half(): pl.pallas_call(mixer_kernel, out_shape=(whole, whole), in_specs=[pl.Block...  16.7 us
    all_to_all x4, starting transfers between devices, over_experts(): lax.all_to_all(pieces, 'ep', split_axis=0, concat_axis=0, tiled=True)  16.2 us
    ppermute x1, waiting for transfers between devices, expert_half(): home_sum = lax.ppermute(far_sum, 'tp', swap)  11.9 us
    dot_general x4, matrix products, down_product(): lax.dot_general(part, piece, (((1,), (1,)), ((), ())), preferred_element_...  11.2 us
    all_gather x1, blocking collectives, entering_2(): packed = lax.all_gather(jnp.stack(x), axis)  10.2 us
    dot_general x2, matrix products, expert_units(): gate_pre = jnp.dot(rows, gate_piece, preferred_element_type=jnp.float32)  9.37 us
  transfers between devices with their start and end apart: 15, of which 6 were waited for; matrix products, arithmetic and copies ran while one was open for 30% of the time, Pallas kernels for 9%

profile of v3, /device:TPU:0, one launch (start us, length us, event | category | flops | bytes accessed | tf_op | source)
XLA Modules:
  0.0 190.4 jit_solution(12961198503459493279)
XLA Ops:
  3.6 4.1 %collective-permute-start.1 = (f32[128,4]{0,1:T(4,128)S(1)}, f32[128,4]{0,1:T(4,128)S(1)}, u32[]{:S(2)}, u32[]{:S(2)}) collective-permute-start(f32[128,4]{0,1:T(4,128)S(1)} %pad_maximum_fusion.5), channel_id=1, source_target_pairs={{0,4},{1,5},{2,6},{3,7},{4,0},{5,1},{6,2},{7,3},{8,12},{9,13},{10,... | collective-permute-start | bytes 6152 | tf_op jit(solution)/shard_map/ppermute | solution.py:244
  12.7 4.5 %all-to-all-start.2 = ((bf16[4,96,2048]{2,1,0:T(8,128)(2,1)}), bf16[4,96,2048]{2,1,0:T(8,128)(2,1)}, u32[]{:S(2)}, u32[]{:S(2)}) async-start(bf16[4,96,2048]{2,1,0:T(8,128)(2,1)} %bitcast.21), calls=%async_computation.2 | async-start | bytes 3145728 | tf_op jit(solution)/shard_map/all_to_all | solution.py:210
  23.6 3.8 %collective-permute-start = (bf16[128,128]{1,0:T(8,128)(2,1)S(1)}, bf16[128,128]{1,0:T(8,128)(2,1)S(1)}, u32[]{:S(2)}, u32[]{:S(2)}) collective-permute-start(bf16[128,128]{1,0:T(8,128)(2,1)S(1)} %slice.79), channel_id=1, source_target_pairs={{0,8},{8,16},{16,24},{1,9},{9,17},{17,25},{2,10},{10,18},{18,26},{... | collective-permute-start | bytes 98312 | tf_op jit(solution)/shard_map/ppermute | solution.py:26
  27.6 7.3 %collective-permute-done.behind_ref = bf16[128,128]{1,0:T(8,128)(2,1)S(1)} collective-permute-done((bf16[128,128]{1,0:T(8,128)(2,1)S(1)}, bf16[128,128]{1,0:T(8,128)(2,1)S(1)}, u32[]{:S(2)}, u32[]{:S(2)}) %collective-permute-start) | collective-permute-done | bytes 32800 | tf_op jit(solution)/shard_map/ppermute | solution.py:26
  34.9 16.7 %shard_map.158 = (f32[128,2048]{1,0:T(8,128)S(1)}, f32[128,2048]{1,0:T(8,128)S(1)}) custom-call(bf16[128,128]{1,0:T(8,128)(2,1)S(1)} %collective-permute-done.behind_ref, bf16[128,2048]{1,0:T(8,128)(2,1)S(1)} %copy-done.1, f32[128,4]{1,0:T(8,128)S(1)} %convert_element_type.101.taps_ref, bf16[256,128]{1,0:T(8,128)(2,1)S(1)} %pad_maximum_fusion.4.maps_ref, ...), custom_call_target="tpu_custom_call" | custom-call | flops 104857600 | bytes 2621440 | tf_op jit(solution)/shard_map/pallas_call | solution.py:140
  52.0 10.2 %all-gather.1 = f32[4,2,128]{2,1,0:T(2,128)S(1)} all-gather(f32[1,2,128]{2,1,0:T(2,128)S(1)} %maximum_bitcast_fusion), channel_id=2, replica_groups=mesh['ep'=4,'tp'=8] {'ep'}, dimensions={0}, use_global_device_ids=true | all-gather | bytes 5120 | tf_op jit(solution)/shard_map/all_gather | solution.py:14
  64.2 4.3 %all-to-all-start.1 = ((bf16[4,96,2048]{2,1,0:T(8,128)(2,1)}), bf16[4,96,2048]{2,1,0:T(8,128)(2,1)}, u32[]{:S(2)}, u32[]{:S(2)}) async-start(bf16[4,96,2048]{2,1,0:T(8,128)(2,1)} %bitcast.114), calls=%async_computation.1 | async-start | bytes 3145728 | tf_op jit(solution)/shard_map/all_to_all | solution.py:210
  71.6 4.6 %collective-permute-done.4 = bf16[2048,256]{1,0:T(8,128)(2,1)} collective-permute-done((bf16[2048,256]{1,0:T(8,128)(2,1)}, bf16[2048,256]{1,0:T(8,128)(2,1)}, u32[]{:S(2)}, u32[]{:S(2)}) %collective-permute-start.4) | collective-permute-done | bytes 1048608 | tf_op jit(solution)/shard_map/ppermute | solution.py:234
  76.2 3.1 %pad_maximum_fusion.2 = bf16[2048,512]{1,0:T(8,128)(2,1)} fusion(bf16[2048,256]{1,0:T(8,128)(2,1)} %collective-permute-done.4, bf16[2048,256]{1,0:T(8,128)(2,1)} %bitcast.24), kind=kLoop, calls=%fused_computation.10 | loop fusion | flops 4194304 | bytes 4194304 | tf_op jit(solution)/shard_map/concatenate | solution.py:237
  80.6 16.7 %collective-permute-done.5 = bf16[2048,256]{1,0:T(8,128)(2,1)} collective-permute-done((bf16[2048,256]{1,0:T(8,128)(2,1)}, bf16[2048,256]{1,0:T(8,128)(2,1)}, u32[]{:S(2)}, u32[]{:S(2)}) %collective-permute-start.5) | collective-permute-done | bytes 1048608 | tf_op jit(solution)/shard_map/ppermute | solution.py:234
  97.2 3.0 %pad_maximum_fusion.3 = bf16[2048,512]{1,0:T(8,128)(2,1)} fusion(bf16[2048,256]{1,0:T(8,128)(2,1)} %collective-permute-done.5, bf16[2048,256]{1,0:T(8,128)(2,1)} %bitcast.25), kind=kLoop, calls=%fused_computation.11 | loop fusion | flops 4194304 | bytes 4194304 | tf_op jit(solution)/shard_map/concatenate | solution.py:237
  100.3 6.0 %all-to-all-start = ((bf16[128,8,256]{2,0,1:T(8,128)(2,1)}), bf16[128,8,256]{2,0,1:T(8,128)(2,1)S(1)}, u32[]{:S(2)}, u32[]{:S(2)}) async-start(bf16[128,8,256]{2,0,1:T(8,128)(2,1)} %bitcast.108), calls=%async_computation | async-start | bytes 1048576 | tf_op jit(solution)/shard_map/all_to_all | solution.py:161
  106.2 4.3 %fusion.54 = f32[768,512]{1,0:T(8,128)S(1)} fusion(bf16[384,2048]{1,0:T(8,128)(2,1)} %bitcast.22, bf16[384,2048]{1,0:T(8,128)(2,1)} %bitcast.19, bf16[2048,256]{1,0:T(8,128)(2,1)} %collective-permute-done.3, bf16[2048,256]{1,0:T(8,128)(2,1)} %bitcast.23), kind=kOutput, calls=%fused_computation.124 | convolution fusion | flops 1621098496 | bytes 6815744 | tf_op jit(solution)/shard_map/dot_general | solution.py:35
  110.5 4.7 %multiply_convert_fusion.1 = bf16[768,512]{1,0:T(8,128)(2,1)S(1)} fusion(f32[768,512]{1,0:T(8,128)S(1)} %fusion.54, bf16[384,2048]{1,0:T(8,128)(2,1)} %bitcast.22, bf16[384,2048]{1,0:T(8,128)(2,1)} %bitcast.19, bf16[2048,256]{1,0:T(8,128)(2,1)} %collective-permute-done.4, bf16[2048,256]{1,0:T(8,128)(2,1)} %bitcast.24), kind=kOutput, calls=%fused_computation.17 | convolution fusion | flops 1625030656 | bytes 7602176 | tf_op jit(solution)/shard_map/dot_general | solution.py:34
  115.2 4.3 %fusion.53 = f32[768,512]{1,0:T(8,128)S(1)} fusion(bf16[2048,512]{1,0:T(8,128)(2,1)} %collective-permute-done.6, bf16[384,2048]{1,0:T(8,128)(2,1)} %bitcast.22, bf16[384,2048]{1,0:T(8,128)(2,1)} %bitcast.19), kind=kOutput, calls=%fused_computation.123 | convolution fusion | flops 1616904192 | bytes 6815744 | tf_op jit(solution)/shard_map/dot_general | solution.py:35
  119.5 4.7 %multiply_convert_fusion = bf16[768,512]{1,0:T(8,128)(2,1)S(1)} fusion(f32[768,512]{1,0:T(8,128)S(1)} %fusion.53, bf16[2048,512]{1,0:T(8,128)(2,1)} %collective-permute-done.7, bf16[384,2048]{1,0:T(8,128)(2,1)} %bitcast.22, bf16[384,2048]{1,0:T(8,128)(2,1)} %bitcast.19), kind=kOutput, calls=%fused_computation.16 | convolution fusion | flops 1620836352 | bytes 7602176 | tf_op jit(solution)/shard_map/dot_general | solution.py:34
  126.5 3.7 %add_convert_fusion = bf16[384,2048]{1,0:T(8,128)(2,1)} fusion(f32[384,2048]{1,0:T(8,128)S(1)} %fusion.20, bf16[768,512]{1,0:T(8,128)(2,1)S(1)} %multiply_convert_fusion.1, bf16[2048,256]{1,0:T(8,128)(2,1)} %collective-permute-done.5, bf16[2048,256]{1,0:T(8,128)(2,1)} %bitcast.25), kind=kOutput, calls=%fused_computation.1 | convolution fusion | flops 811073536 | bytes 7208960 | tf_op jit(solution)/shard_map/dot_general | solution.py:44
  130.2 3.8 %all-to-all-start.4 = ((bf16[4,96,2048]{2,1,0:T(8,128)(2,1)}), bf16[4,96,2048]{2,1,0:T(8,128)(2,1)S(1)}, u32[]{:S(2)}, u32[]{:S(2)}) async-start(bf16[4,96,2048]{2,1,0:T(8,128)(2,1)} %bitcast.116), calls=%async_computation.4 | async-start | bytes 3145728 | tf_op jit(solution)/shard_map/all_to_all | solution.py:210
  136.8 3.7 %add_convert_fusion.1 = bf16[384,2048]{1,0:T(8,128)(2,1)} fusion(f32[384,2048]{1,0:T(8,128)S(1)} %fusion.23, bf16[768,512]{1,0:T(8,128)(2,1)S(1)} %multiply_convert_fusion.1, bf16[2048,256]{1,0:T(8,128)(2,1)} %collective-permute-done.5, bf16[2048,256]{1,0:T(8,128)(2,1)} %bitcast.25), kind=kOutput, calls=%fused_computation.2 | convolution fusion | flops 811073536 | bytes 7208960 | tf_op jit(solution)/shard_map/dot_general | solution.py:44
  140.5 13.4 %all-to-all-done.4 = bf16[4,96,2048]{2,1,0:T(8,128)(2,1)S(1)} async-done(((bf16[4,96,2048]{2,1,0:T(8,128)(2,1)}), bf16[4,96,2048]{2,1,0:T(8,128)(2,1)S(1)}, u32[]{:S(2)}, u32[]{:S(2)}) %all-to-all-start.4) | async-done | bytes 1572896 | tf_op jit(solution)/shard_map/all_to_all | solution.py:210
  153.9 3.6 %all-to-all-start.3 = ((bf16[4,96,2048]{2,1,0:T(8,128)(2,1)}), bf16[4,96,2048]{2,1,0:T(8,128)(2,1)S(1)}, u32[]{:S(2)}, u32[]{:S(2)}) async-start(bf16[4,96,2048]{2,1,0:T(8,128)(2,1)} %bitcast.115), calls=%async_computation.3 | async-start | bytes 3145728 | tf_op jit(solution)/shard_map/all_to_all | solution.py:210
  157.5 4.6 %convolution_convert_fusion.2 = bf16[256,2048]{1,0:T(8,128)(2,1)} fusion(bf16[1024,256]{1,0:T(8,128)(2,1)} %bitcast.118, bf16[1024,2048]{1,0:T(8,128)(2,1)} %param.22), kind=kOutput, calls=%fused_computation.5 | convolution fusion | flops 1074266112 | bytes 5767168 | tf_op jit(solution)/shard_map/dot_general | solution.py:160
  166.4 10.1 %all-to-all-done.3 = bf16[4,96,2048]{2,1,0:T(8,128)(2,1)S(1)} async-done(((bf16[4,96,2048]{2,1,0:T(8,128)(2,1)}), bf16[4,96,2048]{2,1,0:T(8,128)(2,1)S(1)}, u32[]{:S(2)}, u32[]{:S(2)}) %all-to-all-start.3) | async-done | bytes 1572896 | tf_op jit(solution)/shard_map/all_to_all | solution.py:210
  177.5 11.9 %collective-permute-done.9 = bf16[128,2048]{1,0:T(8,128)(2,1)S(1)} collective-permute-done((bf16[128,2048]{1,0:T(8,128)(2,1)}, bf16[128,2048]{1,0:T(8,128)(2,1)S(1)}, u32[]{:S(2)}, u32[]{:S(2)}) %collective-permute-start.9) | collective-permute-done | bytes 524320 | tf_op jit(solution)/shard_map/ppermute | solution.py:268
  (82 shorter events, 32.4 us)
Async XLA Ops:
  0.6 21.9 %copy-start = (bf16[1024,4]{0,1:T(4,128)(2,1)S(1)}, bf16[1024,4]{0,1:T(4,128)(2,1)}, u32[]{:S(2)}) copy-start(bf16[1024,4]{0,1:T(4,128)(2,1)} %param.17) | copy-start | bytes 24580
  3.6 19.9 %collective-permute-start.1 = (f32[128,4]{0,1:T(4,128)S(1)}, f32[128,4]{0,1:T(4,128)S(1)}, u32[]{:S(2)}, u32[]{:S(2)}) collective-permute-start(f32[128,4]{0,1:T(4,128)S(1)} %pad_maximum_fusion.5), channel_id=1, source_target_pairs={{0,4},{1,5},{2,6},{3,7},{4,0},{5,1},{6,2},{7,3},{8,12},{9,13},{10,... | collective-permute-start | bytes 6152 | tf_op jit(solution)/shard_map/ppermute | solution.py:244
  7.7 54.5 %collective-permute-start.2 = (bf16[128,2048]{1,0:T(8,128)(2,1)}, bf16[128,2048]{1,0:T(8,128)(2,1)S(1)}, u32[]{:S(2)}, u32[]{:S(2)}) collective-permute-start(bf16[128,2048]{1,0:T(8,128)(2,1)} %param.23), channel_id=1, source_target_pairs={{0,4},{1,5},{2,6},{3,7},{4,0},{5,1},{6,2},{7,3},{8,12},{9,13},{10,... | collective-permute-start | bytes 1572872 | tf_op jit(solution)/shard_map/ppermute | solution.py:245
  12.7 10.9 %copy-start.1 = (bf16[128,2048]{1,0:T(8,128)(2,1)S(1)}, bf16[128,2048]{1,0:T(8,128)(2,1)}, u32[]{:S(2)}) copy-start(bf16[128,2048]{1,0:T(8,128)(2,1)} %source_ref.1) | copy-start | bytes 1572868
  12.7 22.2 %copy-start.2 = (f32[2048]{0:T(1024)S(1)}, f32[2048]{0:T(1024)}, u32[]{:S(2)}) copy-start(f32[2048]{0:T(1024)} %param.21) | copy-start | bytes 24580
  12.7 51.5 %all-to-all-start.2 = ((bf16[4,96,2048]{2,1,0:T(8,128)(2,1)}), bf16[4,96,2048]{2,1,0:T(8,128)(2,1)}, u32[]{:S(2)}, u32[]{:S(2)}) async-start(bf16[4,96,2048]{2,1,0:T(8,128)(2,1)} %bitcast.21), calls=%async_computation.2 | async-start | bytes 3145728 | tf_op jit(solution)/shard_map/all_to_all | solution.py:210
  17.2 51.4 %collective-permute-start.3 = (bf16[2048,256]{1,0:T(8,128)(2,1)}, bf16[2048,256]{1,0:T(8,128)(2,1)}, u32[]{:S(2)}, u32[]{:S(2)}) collective-permute-start(bf16[2048,256]{1,0:T(8,128)(2,1)} %bitcast.23), channel_id=1, source_target_pairs={{0,2},{1,3},{2,0},{3,1},{4,6},{5,7},{6,4},{7,5},{8,10},{9,11},{10,... | collective-permute-start | bytes 3145736 | tf_op jit(solution)/shard_map/ppermute | solution.py:234
  19.1 57.1 %collective-permute-start.4 = (bf16[2048,256]{1,0:T(8,128)(2,1)}, bf16[2048,256]{1,0:T(8,128)(2,1)}, u32[]{:S(2)}, u32[]{:S(2)}) collective-permute-start(bf16[2048,256]{1,0:T(8,128)(2,1)} %bitcast.24), channel_id=1, source_target_pairs={{0,2},{1,3},{2,0},{3,1},{4,6},{5,7},{6,4},{7,5},{8,10},{9,11},{10,... | collective-permute-start | bytes 3145736 | tf_op jit(solution)/shard_map/ppermute | solution.py:234
  19.3 78.0 %collective-permute-start.5 = (bf16[2048,256]{1,0:T(8,128)(2,1)}, bf16[2048,256]{1,0:T(8,128)(2,1)}, u32[]{:S(2)}, u32[]{:S(2)}) collective-permute-start(bf16[2048,256]{1,0:T(8,128)(2,1)} %bitcast.25), channel_id=1, source_target_pairs={{0,2},{1,3},{2,0},{3,1},{4,6},{5,7},{6,4},{7,5},{8,10},{9,11},{10,... | collective-permute-start | bytes 3145736 | tf_op jit(solution)/shard_map/ppermute | solution.py:234
  23.6 11.3 %collective-permute-start = (bf16[128,128]{1,0:T(8,128)(2,1)S(1)}, bf16[128,128]{1,0:T(8,128)(2,1)S(1)}, u32[]{:S(2)}, u32[]{:S(2)}) collective-permute-start(bf16[128,128]{1,0:T(8,128)(2,1)S(1)} %slice.79), channel_id=1, source_target_pairs={{0,8},{8,16},{16,24},{1,9},{9,17},{17,25},{2,10},{10,18},{18,26},{... | collective-permute-start | bytes 98312 | tf_op jit(solution)/shard_map/ppermute | solution.py:26
  64.2 36.0 %all-to-all-start.1 = ((bf16[4,96,2048]{2,1,0:T(8,128)(2,1)}), bf16[4,96,2048]{2,1,0:T(8,128)(2,1)}, u32[]{:S(2)}, u32[]{:S(2)}) async-start(bf16[4,96,2048]{2,1,0:T(8,128)(2,1)} %bitcast.114), calls=%async_computation.1 | async-start | bytes 3145728 | tf_op jit(solution)/shard_map/all_to_all | solution.py:210
  71.6 7.6 %copy-start.6 = (bf16[128,2048]{1,0:T(8,128)(2,1)S(1)}, bf16[128,2048]{1,0:T(8,128)(2,1)}, u32[]{:S(2)}) copy-start(bf16[128,2048]{1,0:T(8,128)(2,1)} %param.16) | copy-start | bytes 1572868
  71.6 43.6 %collective-permute-start.6 = (bf16[2048,512]{1,0:T(8,128)(2,1)}, bf16[2048,512]{1,0:T(8,128)(2,1)}, u32[]{:S(2)}, u32[]{:S(2)}) collective-permute-start(bf16[2048,512]{1,0:T(8,128)(2,1)} %pad_maximum_fusion.1), channel_id=1, source_target_pairs={{0,1},{1,0},{2,3},{3,2},{4,5},{5,4},{6,7},{7,6},{8,9},{9,8},{10,11... | collective-permute-start | bytes 6291464 | tf_op jit(solution)/shard_map/ppermute | solution.py:234
  79.2 40.3 %collective-permute-start.7 = (bf16[2048,512]{1,0:T(8,128)(2,1)}, bf16[2048,512]{1,0:T(8,128)(2,1)}, u32[]{:S(2)}, u32[]{:S(2)}) collective-permute-start(bf16[2048,512]{1,0:T(8,128)(2,1)} %pad_maximum_fusion.2), channel_id=1, source_target_pairs={{0,1},{1,0},{2,3},{3,2},{4,5},{5,4},{6,7},{7,6},{8,9},{9,8},{10,11... | collective-permute-start | bytes 6291464 | tf_op jit(solution)/shard_map/ppermute | solution.py:234
  100.3 24.0 %collective-permute-start.8 = (bf16[2048,512]{1,0:T(8,128)(2,1)}, bf16[2048,512]{1,0:T(8,128)(2,1)S(1)}, u32[]{:S(2)}, u32[]{:S(2)}) collective-permute-start(bf16[2048,512]{1,0:T(8,128)(2,1)} %pad_maximum_fusion.3), channel_id=1, source_target_pairs={{0,1},{1,0},{2,3},{3,2},{4,5},{5,4},{6,7},{7,6},{8,9},{9,8},{10,11... | collective-permute-start | bytes 6291464 | tf_op jit(solution)/shard_map/ppermute | solution.py:234
  100.3 29.9 %all-to-all-start = ((bf16[128,8,256]{2,0,1:T(8,128)(2,1)}), bf16[128,8,256]{2,0,1:T(8,128)(2,1)S(1)}, u32[]{:S(2)}, u32[]{:S(2)}) async-start(bf16[128,8,256]{2,0,1:T(8,128)(2,1)} %bitcast.108), calls=%async_computation | async-start | bytes 1048576 | tf_op jit(solution)/shard_map/all_to_all | solution.py:161
  124.2 0.9 copy-start.4
  125.1 1.3 copy-start.3
  130.2 3.8 %copy-start.7 = (f32[128,2]{0,1:T(2,128)S(1)}, f32[128,2]{0,1:T(2,128)}, u32[]{:S(2)}) copy-start(f32[128,2]{0,1:T(2,128)} %param.26) | copy-start | bytes 3076
  130.2 6.6 %copy-start.5 = (bf16[128,8,256]{2,0,1:T(8,128)(2,1)}, bf16[128,8,256]{2,0,1:T(8,128)(2,1)S(1)}, u32[]{:S(2)}) copy-start(bf16[128,8,256]{2,0,1:T(8,128)(2,1)S(1)} %all-to-all-done) | copy-start | bytes 1572868
  130.2 23.7 %all-to-all-start.4 = ((bf16[4,96,2048]{2,1,0:T(8,128)(2,1)}), bf16[4,96,2048]{2,1,0:T(8,128)(2,1)S(1)}, u32[]{:S(2)}, u32[]{:S(2)}) async-start(bf16[4,96,2048]{2,1,0:T(8,128)(2,1)} %bitcast.116), calls=%async_computation.4 | async-start | bytes 3145728 | tf_op jit(solution)/shard_map/all_to_all | solution.py:210
  153.9 22.6 %all-to-all-start.3 = ((bf16[4,96,2048]{2,1,0:T(8,128)(2,1)}), bf16[4,96,2048]{2,1,0:T(8,128)(2,1)S(1)}, u32[]{:S(2)}, u32[]{:S(2)}) async-start(bf16[4,96,2048]{2,1,0:T(8,128)(2,1)} %bitcast.115), calls=%async_computation.3 | async-start | bytes 3145728 | tf_op jit(solution)/shard_map/all_to_all | solution.py:210
  163.9 25.6 %collective-permute-start.9 = (bf16[128,2048]{1,0:T(8,128)(2,1)}, bf16[128,2048]{1,0:T(8,128)(2,1)S(1)}, u32[]{:S(2)}, u32[]{:S(2)}) collective-permute-start(bf16[128,2048]{1,0:T(8,128)(2,1)} %add_convert_fusion.3), channel_id=1, source_target_pairs={{0,4},{1,5},{2,6},{3,7},{4,0},{5,1},{6,2},{7,3},{8,12},{9,13},{10,... | collective-permute-start | bytes 1572872 | tf_op jit(solution)/shard_map/ppermute | solution.py:268
